TPU v7x, 32 devices: a whole 2x2x4 slice. The times are simulated.
32 devices in a mesh: sp: 4 (over z), fs: 4 (over y, x), tp: 2 (over core).
Axes of the slice: x: 2, y: 2, z: 4, core: 2. Of those that a mesh axis runs over, the one named last changes fastest.
Arguments:
- inputs: bfloat16 [4, 512, 2048], P('fs', 'sp'), may hold values from -6 to 6
- norm_gain: float32 [2048], replicated, may hold values from 0.1 to 1.9
- w_gate: bfloat16 [2048, 2048], P(('sp', 'fs'), 'tp'), may hold values from -0.125 to 0.125
- w_input: bfloat16 [2048, 2048], P(('sp', 'fs'), 'tp'), may hold values from -0.125 to 0.125
- w_bkey: bfloat16 [2048, 1024], P(('sp', 'fs'), 'tp'), may hold values from -0.125 to 0.125
- w_cquery: bfloat16 [2048, 1024], P(('sp', 'fs'), 'tp'), may hold values from -0.125 to 0.125
- w_step: bfloat16 [2048, 32], replicated, may hold values from -0.125 to 0.125
- conv_weight: float32 [4, 4096], replicated, may hold values from -2 to 2
- decay_rate: float32 [32], replicated, may hold values from 0 to 0.05, as said below
- decay_offset: float32 [4, 512, 32], P('fs', 'sp', 'tp'), may hold values from -2 to 0
- ssd_gain: float32 [2048], replicated, may hold values from 0.1 to 1.9
- w_query: bfloat16 [2048, 2048], P(('sp', 'fs'), 'tp'), may hold values from -0.125 to 0.125
- w_key: bfloat16 [2048, 2048], P(('sp', 'fs'), 'tp'), may hold values from -0.125 to 0.125
- w_value: bfloat16 [2048, 2048], P(('sp', 'fs'), 'tp'), may hold values from -0.125 to 0.125
- stick_bias: float32 [16], replicated, may hold values from -12 to 0
- out_mixer: bfloat16 [2048, 2048], P('tp', ('sp', 'fs')), may hold values from -0.125 to 0.125
- out_attend: bfloat16 [2048, 2048], P('tp', ('sp', 'fs')), may hold values from -3.59375 to 3.59375
Outputs:
- mixed: bfloat16 [4, 512, 2048], P('fs', ('sp', 'tp'))
Inputs may be any that keep to these rules, and one draw needn't show every extreme that they name: `decay_rate`: one positive rate for each head.
All inputs are finite; a program needn't handle non-finite values.
Results may differ from a plain program's by a relative error of at most 0.015.
Values may be sent and summed in bfloat16 or wider, within the bound.
A program may use at most 64 MiB of HBM per device.

v0:
```python
import jax
import jax.numpy as jnp
from jax import lax
from jax.sharding import PartitionSpec as P

HEAD_DIM = 64
STATE = 128
CONV = 4
BLOCK = 128
SB_DIM = 128
SSD_INNER = 2048
GROUP_WIDTH = 1024


EPS = 1e-06


def passed_along(shard, axis, by):
    length = lax.axis_size(axis)
    pairs = [(i, i + by) for i in range(length) if 0 <= i + by < length]
    return lax.ppermute(shard, axis, pairs)


def prefix(shard, axis, join, neutral):
    place = lax.axis_index(axis)
    gathered = jax.tree.map(
        lambda a, kind: lax.all_gather(a.astype(kind), axis), shard, (jnp.bfloat16, jnp.bfloat16)
    )
    state = jax.tree.map(lambda a, e: jnp.zeros_like(a) + jnp.asarray(e, a.dtype), shard, neutral)

    def one(step, state):
        return join(
            state,
            jax.tree.map(
                lambda a, own: lax.dynamic_index_in_dim(a, step, 0, False).astype(own.dtype),
                gathered,
                shard,
            ),
        )

    return lax.fori_loop(0, place, one, state)


def short_conv(rim_rows, current, weights):
    padded = jnp.concatenate([rim_rows, current], axis=0).astype(jnp.float32)
    length = current.shape[0]
    summed = weights[0] * padded[0:length]
    for tap_index in range(1, weights.shape[0]):
        summed = summed + weights[tap_index] * padded[tap_index : tap_index + length]
    return jax.nn.silu(summed).astype(jnp.bfloat16)


def block_terms(input_blocks, bkey_blocks, cquery_blocks, step_blocks, decay_blocks):
    cumulative = jnp.cumsum(decay_blocks, axis=1)
    cum_turned = jnp.transpose(cumulative, (0, 2, 3, 1))
    step_turned = jnp.transpose(step_blocks, (0, 2, 3, 1))
    length = input_blocks.shape[1]
    row_index = lax.broadcasted_iota(jnp.int32, (length, length), 0)
    col_index = lax.broadcasted_iota(jnp.int32, (length, length), 1)
    lower_mask = row_index >= col_index
    spread = cum_turned[..., :, None] - cum_turned[..., None, :]
    inner_prod = jnp.einsum(
        "blgn,bsgn->bgls", cquery_blocks, bkey_blocks, preferred_element_type=jnp.float32
    )
    mixing = jnp.where(
        lower_mask,
        inner_prod[:, :, None]
        * jnp.exp(jnp.where(lower_mask, spread, 0.0))
        * step_turned[..., None, :],
        0.0,
    )
    y_inner = jnp.einsum(
        "bgrls,bsgrp->blgrp",
        mixing.astype(jnp.bfloat16),
        input_blocks,
        preferred_element_type=jnp.float32,
    )
    to_end = jnp.exp(cumulative[:, -1:] - cumulative) * step_blocks
    weighted = (bkey_blocks.astype(jnp.float32)[:, :, :, None, :] * to_end[..., None]).astype(
        jnp.bfloat16
    )
    states = jnp.einsum(
        "blgrp,blgrn->bgrpn", input_blocks, weighted, preferred_element_type=jnp.float32
    )
    return (cumulative, y_inner, states)


def chain_blocks(states, totals):

    def advance(held_state, block_item):
        block_state, block_log = block_item
        return (held_state * jnp.exp(block_log)[..., None, None] + block_state, held_state)

    return lax.scan(advance, jnp.zeros_like(states[0]), (states, totals))


def carried_output(cquery_blocks, entering, cumulative):
    return (
        jnp.einsum(
            "blgn,bgrpn->blgrp",
            cquery_blocks.astype(jnp.float32),
            entering,
            precision=lax.Precision.HIGHEST,
        )
        * jnp.exp(cumulative)[..., None]
    )


def gating_rescaled_output(y_total, gate_act, gain_slice, groups):
    length = y_total.shape[0]
    group_width = y_total.shape[2] * y_total.shape[3]
    gated_out = y_total.reshape(length, groups, group_width) * jax.nn.silu(
        gate_act.astype(jnp.float32)
    ).reshape(length, groups, group_width)
    scaled = gated_out * lax.rsqrt(jnp.mean(gated_out * gated_out, axis=-1, keepdims=True) + EPS)
    return (scaled.reshape(length, groups * group_width) * gain_slice).astype(jnp.bfloat16)


def join_states(earlier, following):
    return (
        earlier[0] * jnp.exp(following[1])[..., None, None] + following[0],
        earlier[1] + following[1],
    )


def stick_piece(carried, query_heads, key_heads, value_heads, bias_heads, causal):
    summed, later_log = carried
    length = query_heads.shape[0]
    key_count = key_heads.shape[0]
    logits = (
        jnp.einsum("thd,shd->hts", query_heads, key_heads, preferred_element_type=jnp.float32)
        * query_heads.shape[2] ** (-0.5)
        + bias_heads[:, None, None]
    )
    log_keep = jax.nn.log_sigmoid(logits)
    log_pass = jax.nn.log_sigmoid(-logits)
    if causal:
        query_pos = lax.broadcasted_iota(jnp.int32, (length, key_count), 0)
        key_pos = lax.broadcasted_iota(jnp.int32, (length, key_count), 1)
        before = key_pos < query_pos
        log_pass = jnp.where(before, log_pass, 0.0)
    tail_sum = lax.cumsum(log_pass, axis=2, reverse=True) - log_pass
    weights = jnp.exp(log_keep + tail_sum + later_log[:, :, None])
    if causal:
        weights = jnp.where(before, weights, 0.0)
    summed = summed + jnp.einsum(
        "hts,shd->thd",
        weights.astype(jnp.bfloat16),
        value_heads,
        preferred_element_type=jnp.float32,
    )
    return (summed, later_log + jnp.sum(log_pass, axis=2))


def body(
    inputs,
    norm_gain,
    w_gate,
    w_input,
    w_bkey,
    w_cquery,
    w_step,
    conv_weight,
    decay_rate,
    decay_offset,
    ssd_gain,
    w_query,
    w_key,
    w_value,
    stick_bias,
    out_mixer,
    out_attend,
):
    tensor_index = lax.axis_index("tp")
    seq_index = lax.axis_index("sp")
    seq_count = lax.axis_size("sp")
    tokens = inputs[0]
    row_count = tokens.shape[0]
    widened = tokens.astype(jnp.float32)
    normed = (
        widened * lax.rsqrt(jnp.mean(widened * widened, axis=-1, keepdims=True) + EPS) * norm_gain
    ).astype(jnp.bfloat16)
    pieces = (
        lax.all_gather(w_gate, ("sp", "fs"), axis=0, tiled=True),
        lax.all_gather(w_input, ("sp", "fs"), axis=0, tiled=True),
        lax.all_gather(w_bkey, ("sp", "fs"), axis=0, tiled=True),
        lax.all_gather(w_cquery, ("sp", "fs"), axis=0, tiled=True),
        lax.all_gather(w_query, ("sp", "fs"), axis=0, tiled=True),
        lax.all_gather(w_key, ("sp", "fs"), axis=0, tiled=True),
        lax.all_gather(w_value, ("sp", "fs"), axis=0, tiled=True),
    )
    projected = tuple(
        (jnp.dot(normed, piece_rows, preferred_element_type=jnp.float32) for piece_rows in pieces)
    )
    gate_act, input_act, input_projection_after_silu, cquery_act, queries, key_act, value_act = (
        tuple((summed.astype(jnp.bfloat16) for summed in projected))
    )
    mixer_full, attend_full = (
        lax.all_gather(out_mixer, ("sp", "fs"), axis=1, tiled=True),
        lax.all_gather(out_attend, ("sp", "fs"), axis=1, tiled=True),
    )
    input_width = input_act.shape[1]
    group_cols = input_projection_after_silu.shape[1]
    heads_local = input_width // HEAD_DIM
    groups_local = group_cols // STATE
    head_ratio = heads_local // groups_local
    blocks_local = row_count // BLOCK
    rim_input, rim_bkey, rim_cquery = passed_along(
        (
            input_act[row_count - CONV + 1 :],
            input_projection_after_silu[row_count - CONV + 1 :],
            cquery_act[row_count - CONV + 1 :],
        ),
        "sp",
        1,
    )
    conv_input = lax.dynamic_slice_in_dim(conv_weight, tensor_index * input_width, input_width, 1)
    conv_bkey = lax.dynamic_slice_in_dim(
        conv_weight, SSD_INNER + tensor_index * group_cols, group_cols, 1
    )
    conv_cquery = lax.dynamic_slice_in_dim(
        conv_weight, SSD_INNER + GROUP_WIDTH + tensor_index * group_cols, group_cols, 1
    )
    input_conv = short_conv(rim_input, input_act, conv_input)
    bkey_conv = short_conv(rim_bkey, input_projection_after_silu, conv_bkey)
    cquery_conv = short_conv(rim_cquery, cquery_act, conv_cquery)
    step_cols = lax.dynamic_slice_in_dim(w_step, tensor_index * heads_local, heads_local, 1)
    step_size = jax.nn.softplus(jnp.dot(normed, step_cols, preferred_element_type=jnp.float32))
    rate_slice = lax.dynamic_slice_in_dim(decay_rate, tensor_index * heads_local, heads_local, 0)
    log_decay = decay_offset[0] - rate_slice * step_size
    input_blocks = input_conv.reshape(blocks_local, BLOCK, groups_local, head_ratio, HEAD_DIM)
    bkey_blocks = bkey_conv.reshape(blocks_local, BLOCK, groups_local, STATE)
    cquery_blocks = cquery_conv.reshape(blocks_local, BLOCK, groups_local, STATE)
    step_blocks = step_size.reshape(blocks_local, BLOCK, groups_local, head_ratio)
    decay_blocks = log_decay.reshape(blocks_local, BLOCK, groups_local, head_ratio)
    cumulative, y_inner, states = block_terms(
        input_blocks, bkey_blocks, cquery_blocks, step_blocks, decay_blocks
    )
    totals = cumulative[:, -1]
    local_end, local_entering = chain_blocks(states, totals)
    device_log = jnp.sum(totals, axis=0)
    carried_state, carried_log = prefix(
        (local_end, device_log),
        "sp",
        join_states,
        (jnp.zeros_like(local_end), jnp.zeros_like(device_log)),
    )
    before_log = jnp.cumsum(totals, axis=0) - totals
    entering = local_entering + jnp.exp(before_log)[..., None, None] * carried_state[None]
    y_total = y_inner + carried_output(cquery_blocks, entering, cumulative)
    gain_slice = lax.dynamic_slice_in_dim(ssd_gain, tensor_index * input_width, input_width, 0)
    y_mixer = gating_rescaled_output(
        y_total.reshape(row_count, groups_local, head_ratio, HEAD_DIM),
        gate_act,
        gain_slice,
        groups_local,
    )
    heads_stick = queries.shape[1] // SB_DIM
    query_heads = queries.reshape(row_count, heads_stick, SB_DIM)
    key_heads = key_act.reshape(row_count, heads_stick, SB_DIM)
    value_heads = value_act.reshape(row_count, heads_stick, SB_DIM)
    bias_heads = lax.dynamic_slice_in_dim(stick_bias, tensor_index * heads_stick, heads_stick, 0)
    carried = (
        jnp.zeros((row_count, heads_stick, SB_DIM), jnp.float32),
        jnp.zeros((heads_stick, row_count), jnp.float32),
    )
    carried = stick_piece(carried, query_heads, key_heads, value_heads, bias_heads, True)

    def relay(turn_index, held_four):
        summed, later_log, key_here, value_here = held_four
        key_here, value_here = passed_along((key_here, value_here), "sp", 1)

        def take_piece(retained_couple):
            return stick_piece(
                retained_couple, query_heads, key_here, value_here, bias_heads, False
            )

        def skip_piece(retained_couple):
            return retained_couple

        summed, later_log = lax.cond(
            turn_index < seq_index, take_piece, skip_piece, (summed, later_log)
        )
        return (summed, later_log, key_here, value_here)

    outcome = lax.fori_loop(
        0, seq_count - 1, relay, (carried[0], carried[1], key_heads, value_heads)
    )
    carried = (outcome[0], outcome[1])
    y_attend = carried[0].astype(jnp.bfloat16).reshape(row_count, heads_stick * SB_DIM)
    mixed = lax.psum_scatter(
        (
            jnp.dot(y_mixer, mixer_full, preferred_element_type=jnp.float32)
            + jnp.dot(y_attend, attend_full, preferred_element_type=jnp.float32)
        ).astype(jnp.bfloat16),
        "tp",
        scatter_dimension=0,
        tiled=True,
    )
    return mixed[None]


def solution(mesh):
    return jax.shard_map(
        body,
        mesh=mesh,
        in_specs=(
            P("fs", "sp", None),
            P(),
            P(("sp", "fs"), "tp"),
            P(("sp", "fs"), "tp"),
            P(("sp", "fs"), "tp"),
            P(("sp", "fs"), "tp"),
            P(),
            P(),
            P(),
            P("fs", "sp", "tp"),
            P(),
            P(("sp", "fs"), "tp"),
            P(("sp", "fs"), "tp"),
            P(("sp", "fs"), "tp"),
            P(),
            P("tp", ("sp", "fs")),
            P("tp", ("sp", "fs")),
        ),
        out_specs=P("fs", ("sp", "tp"), None),
        check_vma=False,
    )
```

profile of v0, /device:TPU:9, one launch (start us, length us, event | category | flops | bytes accessed | tf_op | source)
XLA Modules:
  0.0 761.5 jit_solution(1678125200982186352)
XLA Ops:
  6.6 0.7 all-gather.17.cloned.1.call-update
  7.3 0.7 all-gather.13.cloned.1.call-update
  8.1 0.7 all-gather.15.cloned.1.call-update
  8.8 0.5 all-gather.27.cloned.1.call-update
  9.4 0.5 all-gather.25.cloned.1.call-update
  10.0 0.5 all-gather.23.cloned.1.call-update
  10.5 0.7 all-gather.19.cloned.1.call-update
  11.3 0.7 dynamic_slice.40
  12.0 1.2 fusion.26
  13.3 1.4 bitcast_subtract_fusion.1
  15.3 55.4 %all-gather.17.cloned.1.call-done = bf16[2048,512]{1,0:T(8,128)(2,1)} async-done(((bf16[128,512]{1,0:T(8,128)(2,1)}), bf16[2048,512]{1,0:T(8,128)(2,1)}) %all-gather.17.cloned.1.call-update) | async-done | bytes 2097168 | tf_op jit(solution)/shard_map/all_gather | solution.py:186
  70.7 2.1 convolution_convert_fusion.5
  72.8 2.6 collective-permute-start.4
  75.6 1.6 collective-permute-done.4
  77.2 70.5 %all-gather.13.cloned.1.call-done = bf16[2048,1024]{1,0:T(8,128)(2,1)} async-done(((bf16[128,1024]{1,0:T(8,128)(2,1)}), bf16[2048,1024]{1,0:T(8,128)(2,1)}) %all-gather.13.cloned.1.call-update) | async-done | bytes 4194320 | tf_op jit(solution)/shard_map/all_gather | solution.py:185
  147.7 2.9 convolution_convert_fusion.4
  150.7 3.1 collective-permute-start.2
  154.0 1.0 collective-permute-done.2
  155.6 1.2 fusion.21
  157.0 0.7 all-gather.21.cloned.1.call-update
  157.7 0.5 all-gather.29.cloned.1.call-update
  158.3 51.4 %all-gather.15.cloned.1.call-done = bf16[2048,512]{1,0:T(8,128)(2,1)} async-done(((bf16[128,512]{1,0:T(8,128)(2,1)}), bf16[2048,512]{1,0:T(8,128)(2,1)}) %all-gather.15.cloned.1.call-update) | async-done | bytes 2097168 | tf_op jit(solution)/shard_map/all_gather | solution.py:187
  209.7 2.1 convolution_convert_fusion.6
  211.8 2.6 collective-permute-start.3
  214.4 6.8 all-gather
  221.7 1.2 fusion.61
  222.9 63.7 %all-gather.27.cloned.1.call-done = bf16[2048,1024]{1,0:T(8,128)(2,1)} async-done(((bf16[128,1024]{1,0:T(8,128)(2,1)}), bf16[2048,1024]{1,0:T(8,128)(2,1)}) %all-gather.27.cloned.1.call-update) | async-done | bytes 4194320 | tf_op jit(solution)/shard_map/all_gather | solution.py:189
  286.5 3.0 fusion.25
  289.5 73.8 %all-gather.25.cloned.1.call-done = bf16[2048,1024]{1,0:T(8,128)(2,1)} async-done(((bf16[128,1024]{1,0:T(8,128)(2,1)}), bf16[2048,1024]{1,0:T(8,128)(2,1)}) %all-gather.25.cloned.1.call-update) | async-done | bytes 4194320 | tf_op jit(solution)/shard_map/all_gather | solution.py:188
  363.4 3.0 fusion.24
  366.4 73.8 %all-gather.23.cloned.1.call-done = bf16[2048,1024]{1,0:T(8,128)(2,1)} async-done(((bf16[128,1024]{1,0:T(8,128)(2,1)}), bf16[2048,1024]{1,0:T(8,128)(2,1)}) %all-gather.23.cloned.1.call-update) | async-done | bytes 4194320 | tf_op jit(solution)/shard_map/all_gather | solution.py:190
  440.2 3.0 fusion.23
  443.6 0.4 fusion.76
  443.9 1.3 fusion.37
  445.2 0.9 convolution_bitcast_fusion.1
  446.4 85.5 %while.37 = (s32[]{:T(128)}, f32[128,8,128]{2,0,1:T(8,128)S(1)}, f32[8,128]{1,0:T(8,128)S(1)}, bf16[128,8,128]{2,0,1:T(8,128)(2,1)S(1)}, bf16[128,8,128]{2,0,1:T...) while((s32[]{:T(128)}, f32[128,8,128]{2,0,1:T(8,128)S(1)}, ...), condition=%wide.region_12.13_spmd, body=%wide.region_7.12_spmd.sunk | while | flops 89113600 | bytes 8720691 | solution.py:286
  446.4 3.1 collective-permute-start
  449.5 2.2 collective-permute-start.1
  451.7 3.7 collective-permute-done
  455.3 10.3 %collective-permute-done.1 = bf16[128,8,128]{2,0,1:T(8,128)(2,1)S(1)} collective-permute-done((bf16[128,8,128]{2,0,1:T(8,128)(2,1)S(1)}, bf16[128,8,128]{2,0,1:T(8,128)(2,1)S(1)}, u32[]{:S(2)}, u32[]{:S(2)}) %collective-permute-start.1) | collective-permute-done | bytes 262176 | tf_op jit(solution)/shard_map/while/body/eval_jaxpr/ppermute | solution.py:21
  465.6 2.9 conditional.2
  465.9 0.3 fusion.12
  466.3 1.3 fusion.7
  467.6 0.9 fusion
  468.6 3.4 collective-permute-start
  472.0 2.2 collective-permute-start.1
  474.2 10.7 %collective-permute-done = bf16[128,8,128]{2,0,1:T(8,128)(2,1)S(1)} collective-permute-done((bf16[128,8,128]{2,0,1:T(8,128)(2,1)S(1)}, bf16[128,8,128]{2,0,1:T(8,128)(2,1)S(1)}, u32[]{:S(2)}, u32[]{:S(2)}) %collective-permute-start) | collective-permute-done | bytes 262176 | tf_op jit(solution)/shard_map/while/body/eval_jaxpr/ppermute | solution.py:21
  484.9 8.6 %collective-permute-done.1 = bf16[128,8,128]{2,0,1:T(8,128)(2,1)S(1)} collective-permute-done((bf16[128,8,128]{2,0,1:T(8,128)(2,1)S(1)}, bf16[128,8,128]{2,0,1:T(8,128)(2,1)S(1)}, u32[]{:S(2)}, u32[]{:S(2)}) %collective-permute-start.1) | collective-permute-done | bytes 262176 | tf_op jit(solution)/shard_map/while/body/eval_jaxpr/ppermute | solution.py:21
  493.5 6.4 collective-permute-start
  500.0 3.4 collective-permute-start.1
  503.4 10.3 %collective-permute-done = bf16[128,8,128]{2,0,1:T(8,128)(2,1)S(1)} collective-permute-done((bf16[128,8,128]{2,0,1:T(8,128)(2,1)S(1)}, bf16[128,8,128]{2,0,1:T(8,128)(2,1)S(1)}, u32[]{:S(2)}, u32[]{:S(2)}) %collective-permute-start) | collective-permute-done | bytes 262176 | tf_op jit(solution)/shard_map/while/body/eval_jaxpr/ppermute | solution.py:21
  513.7 18.1 %collective-permute-done.1 = bf16[128,8,128]{2,0,1:T(8,128)(2,1)S(1)} collective-permute-done((bf16[128,8,128]{2,0,1:T(8,128)(2,1)S(1)}, bf16[128,8,128]{2,0,1:T(8,128)(2,1)S(1)}, u32[]{:S(2)}, u32[]{:S(2)}) %collective-permute-start.1) | collective-permute-done | bytes 262176 | tf_op jit(solution)/shard_map/while/body/eval_jaxpr/ppermute | solution.py:21
  532.1 0.5 all-gather.19.cloned.1.call-done
  532.5 3.0 divide_multiply_fusion
  535.8 27.3 %all-gather.31.cloned.1.call-done = bf16[16,4,64,128]{3,2,1,0:T(8,128)(2,1)} async-done(((bf16[4,4,64,128]{3,2,1,0:T(8,128)(2,1)}), bf16[16,4,64,128]{3,2,1,0:T(8,128)(2,1)}) %all-gather.31.cloned.1.call-update) | async-done | bytes 1048592 | tf_op jit(solution)/shard_map/all_gather | solution.py:27
  563.1 1.4 while.36
  563.1 1.1 convert_add_fusion.2
  564.5 0.4 fusion.20
  565.0 1.5 multiply_reduce_fusion
  567.1 85.0 %all-gather.21.cloned.1.call-done = bf16[1024,2048]{1,0:T(8,128)(2,1)} async-done(((bf16[1024,128]{1,0:T(8,128)(2,1)}), bf16[1024,2048]{1,0:T(8,128)(2,1)}) %all-gather.21.cloned.1.call-update) | async-done | bytes 4194320 | tf_op jit(solution)/shard_map/all_gather | solution.py:199
  652.2 2.9 fusion.48
  655.1 86.5 %all-gather.29.cloned.1.call-done = bf16[1024,2048]{1,0:T(8,128)(2,1)} async-done(((bf16[1024,128]{1,0:T(8,128)(2,1)}), bf16[1024,2048]{1,0:T(8,128)(2,1)}) %all-gather.29.cloned.1.call-update) | async-done | bytes 4194320 | tf_op jit(solution)/shard_map/all_gather | solution.py:200
  741.6 3.8 fusion.17
  745.4 9.6 %reduce-scatter.2.cloned.1.call-done = bf16[64,2048]{1,0:T(8,128)(2,1)} async-done(((bf16[128,2048]{1,0:T(8,128)(2,1)}), bf16[64,2048]{1,0:T(8,128)(2,1)}) %reduce-scatter.2.cloned.1.call-update) | async-done | bytes 262160 | tf_op jit(solution)/shard_map/reduce_scatter | solution.py:291
  (77 shorter events, 4.7 us)
Async XLA Ops:
  6.5 6.7 copy-start
  6.5 64.2 %copy-start.1 = (bf16[1,128,2048]{2,1,0:T(8,128)(2,1)S(1)}, bf16[1,128,2048]{2,1,0:T(8,128)(2,1)}, u32[]{:S(2)}) copy-start(bf16[1,128,2048]{2,1,0:T(8,128)(2,1)} %param.23) | copy-start | bytes 1572868
  6.5 64.2 %copy-start.2 = (f32[2048]{0:T(1024)S(1)}, f32[2048]{0:T(1024)}, u32[]{:S(2)}) copy-start(f32[2048]{0:T(1024)} %param.24) | copy-start | bytes 24580
  6.5 8.6 %copy-start.3 = (f32[4,4096]{1,0:T(4,128)S(1)}, f32[4,4096]{1,0:T(4,128)}, u32[]{:S(2)}) copy-start(f32[4,4096]{1,0:T(4,128)} %param.30) | copy-start | bytes 196612
  6.5 64.2 %all-gather.17.cloned.1.call-start = ((), (), s32[]{:S(2)}) async-start(), calls=%async_computation.3 | async-start | bytes 2228224 | tf_op jit(solution)/shard_map/all_gather | solution.py:186
  7.3 140.4 %all-gather.13.cloned.1.call-start = ((), (), s32[]{:S(2)}) async-start(), calls=%async_computation.1 | async-start | bytes 4456448 | tf_op jit(solution)/shard_map/all_gather | solution.py:185
  8.0 201.7 %all-gather.15.cloned.1.call-start = ((), (), s32[]{:S(2)}) async-start(), calls=%async_computation.2 | async-start | bytes 2228224 | tf_op jit(solution)/shard_map/all_gather | solution.py:187
  8.8 277.8 %all-gather.27.cloned.1.call-start = ((), (), s32[]{:S(2)}) async-start(), calls=%async_computation.8 | async-start | bytes 4456448 | tf_op jit(solution)/shard_map/all_gather | solution.py:189
  9.3 354.0 %all-gather.25.cloned.1.call-start = ((), (), s32[]{:S(2)}) async-start(), calls=%async_computation.7 | async-start | bytes 4456448 | tf_op jit(solution)/shard_map/all_gather | solution.py:188
  9.9 430.3 %all-gather.23.cloned.1.call-start = ((), (), s32[]{:S(2)}) async-start(), calls=%async_computation.6 | async-start | bytes 4456448 | tf_op jit(solution)/shard_map/all_gather | solution.py:190
  10.5 522.0 %all-gather.19.cloned.1.call-start = ((), (), s32[]{:S(2)}) async-start(), calls=%async_computation.4 | async-start | bytes 4456448 | tf_op jit(solution)/shard_map/all_gather | solution.py:184
  11.2 551.8 %all-gather.31.cloned.1.call-start = ((), (), s32[]{:S(2)}) async-start(), calls=%async_computation.11 | async-start | bytes 1310720 | tf_op jit(solution)/shard_map/all_gather | solution.py:27
  72.8 4.4 collective-permute-start.4
  150.7 4.4 collective-permute-start.2
  154.0 67.3 %copy-start.4 = (f32[16]{0:T(128)S(1)}, f32[16]{0:T(128)}, u32[]{:S(2)}) copy-start(f32[16]{0:T(128)} %param.37) | copy-start | bytes 196
  156.9 495.2 %all-gather.21.cloned.1.call-start = ((), (), s32[]{:S(2)}) async-start(), calls=%async_computation.5 | async-start | bytes 4456448 | tf_op jit(solution)/shard_map/all_gather | solution.py:199
  157.6 584.0 %all-gather.29.cloned.1.call-start = ((), (), s32[]{:S(2)}) async-start(), calls=%async_computation.9 | async-start | bytes 4456448 | tf_op jit(solution)/shard_map/all_gather | solution.py:200
  158.2 596.8 %reduce-scatter.2.cloned.1.call-start = ((), (), s32[]{:S(2)}) async-start(), calls=%async_computation.10 | async-start | bytes 786432 | tf_op jit(solution)/shard_map/reduce_scatter | solution.py:291
  211.8 9.6 %collective-permute-start.3 = (bf16[3,512]{1,0:T(4,128)(2,1)S(1)}, bf16[3,512]{1,0:T(4,128)(2,1)S(1)}, u32[]{:S(2)}, u32[]{:S(2)}) collective-permute-start(bf16[3,512]{1,0:T(4,128)(2,1)S(1)} %slice.118), channel_id=1, source_target_pairs={{0,8},{8,16},{16,24},{1,9},{9,17},{17,25},{2,10},{10,18},{18,26},{... | collective-permute-start | bytes 9224 | tf_op jit(solution)/shard_map/ppermute | solution.py:21
  446.4 9.0 %collective-permute-start = (bf16[128,8,128]{2,0,1:T(8,128)(2,1)S(1)}, bf16[128,8,128]{2,0,1:T(8,128)(2,1)S(1)}, u32[]{:S(2)}, u32[]{:S(2)}) collective-permute-start(bf16[128,8,128]{2,0,1:T(8,128)(2,1)S(1)} %get-tuple-element.444), channel_id=1, source_target_pairs={{0,8},{8,16},{16,24},{1,9},{9,17},{17,25},{2,10},{10,18},{18,26},{... | collective-permute-start | bytes 786440 | tf_op jit(solution)/shard_map/while/body/eval_jaxpr/ppermute | solution.py:21
  449.5 16.1 %collective-permute-start.1 = (bf16[128,8,128]{2,0,1:T(8,128)(2,1)S(1)}, bf16[128,8,128]{2,0,1:T(8,128)(2,1)S(1)}, u32[]{:S(2)}, u32[]{:S(2)}) collective-permute-start(bf16[128,8,128]{2,0,1:T(8,128)(2,1)S(1)} %get-tuple-element.445), channel_id=1, source_target_pairs={{0,8},{8,16},{16,24},{1,9},{9,17},{17,25},{2,10},{10,18},{18,26},{... | collective-permute-start | bytes 786440 | tf_op jit(solution)/shard_map/while/body/eval_jaxpr/ppermute | solution.py:21
  468.6 16.3 %collective-permute-start = (bf16[128,8,128]{2,0,1:T(8,128)(2,1)S(1)}, bf16[128,8,128]{2,0,1:T(8,128)(2,1)S(1)}, u32[]{:S(2)}, u32[]{:S(2)}) collective-permute-start(bf16[128,8,128]{2,0,1:T(8,128)(2,1)S(1)} %get-tuple-element.444), channel_id=1, source_target_pairs={{0,8},{8,16},{16,24},{1,9},{9,17},{17,25},{2,10},{10,18},{18,26},{... | collective-permute-start | bytes 786440 | tf_op jit(solution)/shard_map/while/body/eval_jaxpr/ppermute | solution.py:21
  472.0 21.4 %collective-permute-start.1 = (bf16[128,8,128]{2,0,1:T(8,128)(2,1)S(1)}, bf16[128,8,128]{2,0,1:T(8,128)(2,1)S(1)}, u32[]{:S(2)}, u32[]{:S(2)}) collective-permute-start(bf16[128,8,128]{2,0,1:T(8,128)(2,1)S(1)} %get-tuple-element.445), channel_id=1, source_target_pairs={{0,8},{8,16},{16,24},{1,9},{9,17},{17,25},{2,10},{10,18},{18,26},{... | collective-permute-start | bytes 786440 | tf_op jit(solution)/shard_map/while/body/eval_jaxpr/ppermute | solution.py:21
  493.5 20.1 %collective-permute-start = (bf16[128,8,128]{2,0,1:T(8,128)(2,1)S(1)}, bf16[128,8,128]{2,0,1:T(8,128)(2,1)S(1)}, u32[]{:S(2)}, u32[]{:S(2)}) collective-permute-start(bf16[128,8,128]{2,0,1:T(8,128)(2,1)S(1)} %get-tuple-element.444), channel_id=1, source_target_pairs={{0,8},{8,16},{16,24},{1,9},{9,17},{17,25},{2,10},{10,18},{18,26},{... | collective-permute-start | bytes 786440 | tf_op jit(solution)/shard_map/while/body/eval_jaxpr/ppermute | solution.py:21
  500.0 31.9 %collective-permute-start.1 = (bf16[128,8,128]{2,0,1:T(8,128)(2,1)S(1)}, bf16[128,8,128]{2,0,1:T(8,128)(2,1)S(1)}, u32[]{:S(2)}, u32[]{:S(2)}) collective-permute-start(bf16[128,8,128]{2,0,1:T(8,128)(2,1)S(1)} %get-tuple-element.445), channel_id=1, source_target_pairs={{0,8},{8,16},{16,24},{1,9},{9,17},{17,25},{2,10},{10,18},{18,26},{... | collective-permute-start | bytes 786440 | tf_op jit(solution)/shard_map/while/body/eval_jaxpr/ppermute | solution.py:21
  564.5 87.7 %dynamic-slice-start = ((f32[2048]{0:T(1024)}, s32[]{:T(128)}), f32[1024]{0:T(1024)S(1)}, s32[]{:S(2)}) async-start(f32[2048]{0:T(1024)} %param.33, s32[]{:T(128)} %select_n.71), calls=%async_computation.12 | async-start | bytes 8704 | tf_op jit(solution)/shard_map/dynamic_slice | solution.py:251
Sparse Core Ops, SparseCore 0:
  10.1 60.5 all-gather.16
  73.5 74.1 all-gather.12
  150.5 59.1 all-gather.14
  212.3 74.1 all-gather.26
  289.1 74.1 all-gather.24
  366.0 74.1 all-gather.22
  443.0 89.5 all-gather.18
  534.1 28.8 all-gather.30
  565.8 86.3 all-gather.20
  654.7 86.8 all-gather.28
  745.5 9.3 reduce-scatter.1
where the time goes:
time: 763 us; the launch traced here: 762 us
  waiting for transfers between devices  667 us (87%)
  matrix products  34 us (4%)
  starting transfers between devices  29.4 us (4%)
  between operations  13.6 us (2%)
    all_gather x1, waiting for transfers between devices, body(): lax.all_gather(out_attend, ('sp', 'fs'), axis=1, tiled=True)  86.5 us
    all_gather x1, waiting for transfers between devices, body(): lax.all_gather(out_mixer, ('sp', 'fs'), axis=1, tiled=True)  85 us
    all_gather x1, waiting for transfers between devices, body(): lax.all_gather(w_value, ('sp', 'fs'), axis=0, tiled=True)  73.8 us
    all_gather x1, waiting for transfers between devices, body(): lax.all_gather(w_query, ('sp', 'fs'), axis=0, tiled=True)  73.8 us
    all_gather x1, waiting for transfers between devices, body(): lax.all_gather(w_input, ('sp', 'fs'), axis=0, tiled=True)  70.5 us
    ppermute x9, waiting for transfers between devices, passed_along(): return lax.ppermute(shard, axis, pairs)  64.3 us
    all_gather x1, waiting for transfers between devices, body(): lax.all_gather(w_key, ('sp', 'fs'), axis=0, tiled=True)  63.7 us
    all_gather x1, waiting for transfers between devices, body(): lax.all_gather(w_bkey, ('sp', 'fs'), axis=0, tiled=True)  55.4 us
  transfers between devices with their start and end apart: 20, of which 19 were waited for; matrix products, arithmetic and copies ran while one was open for 5% of the time, Pallas kernels for 0%

commit v1 on v0

--- a/solution.py
+++ b/solution.py
@@ -300,9 +300,143 @@
     return mixed[None]
 
 
+def stick_heads(query_heads, key_heads, value_heads, bias_heads):
+    length = query_heads.shape[0]
+    logits = (
+        jnp.einsum("thd,shd->hts", query_heads, key_heads, preferred_element_type=jnp.float32)
+        * query_heads.shape[2] ** (-0.5)
+        + bias_heads[:, None, None]
+    )
+    row_index = lax.broadcasted_iota(jnp.int32, (length, length), 0)
+    col_index = lax.broadcasted_iota(jnp.int32, (length, length), 1)
+    before = col_index < row_index
+    log_keep = jax.nn.log_sigmoid(logits)
+    log_pass = jnp.where(before, log_keep - logits, 0.0)
+    later = (row_index > col_index).astype(jnp.float32)
+    tail_sum = jnp.einsum("htr,rs->hts", log_pass, later, precision=lax.Precision.HIGHEST)
+    weights = jnp.where(before, jnp.exp(log_keep + tail_sum), 0.0)
+    return jnp.einsum(
+        "hts,shd->thd",
+        weights.astype(jnp.bfloat16),
+        value_heads,
+        preferred_element_type=jnp.float32,
+    ).astype(jnp.bfloat16)
+
+
+def head_body(
+    inputs,
+    norm_gain,
+    w_gate,
+    w_input,
+    w_bkey,
+    w_cquery,
+    w_step,
+    conv_weight,
+    decay_rate,
+    decay_offset,
+    ssd_gain,
+    w_query,
+    w_key,
+    w_value,
+    stick_bias,
+    out_mixer,
+    out_attend,
+):
+    seq_count = lax.axis_size("sp")
+    batch_count = lax.axis_size("fs")
+    place = lax.axis_index("tp") * seq_count + lax.axis_index("sp")
+    tokens = inputs[0]
+    row_count, width = tokens.shape
+    widened = tokens.astype(jnp.float32)
+    normed = (
+        widened * lax.rsqrt(jnp.mean(widened * widened, axis=-1, keepdims=True) + EPS) * norm_gain
+    ).astype(jnp.bfloat16)
+    weights = (w_gate, w_input, w_bkey, w_cquery, w_query, w_key, w_value)
+    depth = w_gate.shape[0]
+    widths = [w.shape[1] // seq_count for w in weights]
+    packed = jnp.concatenate([w.reshape(depth, seq_count, -1) for w in weights], axis=2)
+    packed = jnp.transpose(packed, (1, 0, 2))
+    packed_out = jnp.concatenate(
+        [w.reshape(seq_count, -1, w.shape[1]) for w in (out_mixer, out_attend)], axis=1
+    )
+    normed = lax.all_gather(normed, "sp", axis=0, tiled=True)
+    offset = lax.all_to_all(
+        decay_offset[0].reshape(row_count, seq_count, -1), "sp", 1, 0, tiled=True
+    )
+    length = normed.shape[0]
+    offset = offset.reshape(length, -1)
+    packed = lax.all_to_all(packed, "sp", 0, 0, tiled=True)
+    packed_out = lax.all_to_all(packed_out, "sp", 0, 0, tiled=True)
+    packed = lax.all_gather(packed, "fs", axis=1)
+    packed_out = lax.all_gather(packed_out, "fs", axis=1)
+    rows = packed.reshape(width, -1)
+    projected = jnp.dot(normed, rows, preferred_element_type=jnp.float32).astype(jnp.bfloat16)
+    acts = []
+    start = 0
+    for w in widths:
+        acts.append(projected[:, start : start + w])
+        start += w
+    gate_act, input_act, bkey_act, cquery_act, queries, key_act, value_act = acts
+    input_width = input_act.shape[1]
+    group_cols = bkey_act.shape[1]
+    heads_local = input_width // HEAD_DIM
+    groups_local = group_cols // STATE
+    head_ratio = heads_local // groups_local
+    blocks_local = length // BLOCK
+
+    def conv(act, first):
+        taps = lax.dynamic_slice_in_dim(
+            conv_weight, first + place * act.shape[1], act.shape[1], 1
+        )
+        return short_conv(jnp.zeros((CONV - 1, act.shape[1]), act.dtype), act, taps)
+
+    input_conv = conv(input_act, 0)
+    bkey_conv = conv(bkey_act, SSD_INNER)
+    cquery_conv = conv(cquery_act, SSD_INNER + GROUP_WIDTH)
+    step_cols = lax.dynamic_slice_in_dim(w_step, place * heads_local, heads_local, 1)
+    step_size = jax.nn.softplus(jnp.dot(normed, step_cols, preferred_element_type=jnp.float32))
+    rate_slice = lax.dynamic_slice_in_dim(decay_rate, place * heads_local, heads_local, 0)
+    log_decay = offset - rate_slice * step_size
+    input_blocks = input_conv.reshape(blocks_local, BLOCK, groups_local, head_ratio, HEAD_DIM)
+    bkey_blocks = bkey_conv.reshape(blocks_local, BLOCK, groups_local, STATE)
+    cquery_blocks = cquery_conv.reshape(blocks_local, BLOCK, groups_local, STATE)
+    step_blocks = step_size.reshape(blocks_local, BLOCK, groups_local, head_ratio)
+    decay_blocks = log_decay.reshape(blocks_local, BLOCK, groups_local, head_ratio)
+    cumulative, y_inner, states = block_terms(
+        input_blocks, bkey_blocks, cquery_blocks, step_blocks, decay_blocks
+    )
+    _, entering = chain_blocks(states, cumulative[:, -1])
+    y_total = y_inner + carried_output(cquery_blocks, entering, cumulative)
+    gain_slice = lax.dynamic_slice_in_dim(ssd_gain, place * input_width, input_width, 0)
+    y_mixer = gating_rescaled_output(
+        y_total.reshape(length, groups_local, head_ratio, HEAD_DIM),
+        gate_act,
+        gain_slice,
+        groups_local,
+    )
+    heads_stick = queries.shape[1] // SB_DIM
+    bias_heads = lax.dynamic_slice_in_dim(stick_bias, place * heads_stick, heads_stick, 0)
+    y_attend = stick_heads(
+        queries.reshape(length, heads_stick, SB_DIM),
+        key_act.reshape(length, heads_stick, SB_DIM),
+        value_act.reshape(length, heads_stick, SB_DIM),
+        bias_heads,
+    ).reshape(length, heads_stick * SB_DIM)
+    y_both = jnp.concatenate([y_mixer, y_attend], axis=1)
+    out_rows = jnp.transpose(packed_out, (2, 0, 1, 3)).reshape(y_both.shape[1], -1)
+    share = jnp.dot(y_both, out_rows, preferred_element_type=jnp.float32).astype(jnp.bfloat16)
+    mixed = lax.psum_scatter(share, ("sp", "tp"), scatter_dimension=0, tiled=True)
+    return mixed[None]
+
+
+def by_heads(mesh):
+    groups = GROUP_WIDTH // STATE
+    return groups % (mesh.shape["tp"] * mesh.shape["sp"]) == 0
+
+
 def solution(mesh):
     return jax.shard_map(
-        body,
+        head_body if by_heads(mesh) else body,
         mesh=mesh,
         in_specs=(
             P("fs", "sp", None),

time: 763 us -> 284 us (0.37)
  the two profiles are of different devices: /device:TPU:9 before, /device:TPU:0 now
where the time goes in v1:
time: 284 us; the launch traced here: 283 us
  waiting for transfers between devices  146 us (51%)
  blocking collectives  54.3 us (19%)
  local copies, waits for them, and re-layouts  27.2 us (10%)
  matrix products  24.1 us (8%)
  between operations  13.6 us (5%)
  starting transfers between devices  9.86 us (3%)
  other arithmetic  7.58 us (3%)
    all_gather x1, waiting for transfers between devices, head_body(): packed = lax.all_gather(packed, 'fs', axis=1)  67.5 us
    all_to_all x1, blocking collectives, head_body(): packed = lax.all_to_all(packed, 'sp', 0, 0, tiled=True)  54.3 us
    reduce_scatter x1, waiting for transfers between devices, head_body(): lax.psum_scatter(share, ('sp', 'tp'), scatter_dimension=0, tiled=True)  36.2 us
    all_to_all x1, waiting for transfers between devices, head_body(): packed_out = lax.all_to_all(packed_out, 'sp', 0, 0, tiled=True)  25.4 us
    all_gather x1, waiting for transfers between devices, head_body(): packed_out = lax.all_gather(packed_out, 'fs', axis=1)  16.3 us
    all_gather x1, local copies, waits for them, and re-layouts, head_body(): packed = lax.all_gather(packed, 'fs', axis=1)  8.64 us
    dot_general x1, matrix products, head_body(): jnp.dot(normed, rows, preferred_element_type=jnp.float32)  6.83 us
    all_to_all x1, starting transfers between devices, head_body(): packed_out = lax.all_to_all(packed_out, 'sp', 0, 0, tiled=True)  6.48 us
  transfers between devices with their start and end apart: 6, of which 5 were waited for; matrix products, arithmetic and copies ran while one was open for 6% of the time, Pallas kernels for 0%

profile of v1, /device:TPU:0, one launch (start us, length us, event | category | flops | bytes accessed | tf_op | source)
XLA Modules:
  0.0 282.8 jit_solution(13797762285959471221)
XLA Ops:
  6.6 1.3 fusion.10
  7.9 2.1 fusion.12
  10.1 0.8 pad_maximum_fusion
  10.9 6.5 %all-to-all-start.2 = ((bf16[4,512,128]{2,1,0:T(8,128)(2,1)}), bf16[4,512,128]{2,1,0:T(8,128)(2,1)S(1)}, u32[]{:S(2)}, u32[]{:S(2)}) async-start(bf16[4,512,128]{2,1,0:T(8,128)(2,1)} %pad_maximum_fusion), calls=%async_computation.2 | async-start | bytes 1048576 | tf_op jit(solution)/shard_map/all_to_all | solution.py:369
  17.4 0.2 copy.109
  17.6 0.2 copy.110
  17.8 0.1 copy.111
  17.9 0.1 copy.112
  18.0 0.2 copy.113
  18.2 0.2 copy.114
  18.4 0.2 copy.115
  18.6 25.4 %all-to-all-done.2 = bf16[4,512,128]{2,1,0:T(8,128)(2,1)S(1)} async-done(((bf16[4,512,128]{2,1,0:T(8,128)(2,1)}), bf16[4,512,128]{2,1,0:T(8,128)(2,1)S(1)}, u32[]{:S(2)}, u32[]{:S(2)}) %all-to-all-start.2) | async-done | bytes 524320 | tf_op jit(solution)/shard_map/all_to_all | solution.py:369
  44.0 0.8 copy-done.1
  45.2 54.3 %all_to_all.25 = bf16[4,128,1536]{1,2,0:T(8,128)(2,1)} all-to-all(bf16[4,128,1536]{1,2,0:T(8,128)(2,1)S(1)} %bitcast.144), channel_id=1, replica_groups=mesh['sp'=4,'fs'=4,'tp'=2] {'sp'}, dimensions={0} | all-to-all | bytes 3145728 | tf_op jit(solution)/shard_map/all_to_all | solution.py:368
  99.5 3.3 %all-to-all-start.1 = ((f32[128,4,4]{0,2,1:T(4,128)}), f32[128,4,4]{0,2,1:T(4,128)S(1)}, u32[]{:S(2)}, u32[]{:S(2)}) async-start(f32[128,4,4]{0,2,1:T(4,128)} %bitcast.25), calls=%async_computation.1 | async-start | bytes 16384 | tf_op jit(solution)/shard_map/all_to_all | solution.py:363
  102.9 0.7 constant_dynamic-slice_fusion.2
  103.6 0.6 iota_compare_fusion.2
  104.2 0.8 iota_compare_fusion.1
  105.0 0.9 constant_dynamic-slice_fusion.1
  106.0 1.3 dynamic_slice.34
  107.3 0.6 dynamic_slice.35
  107.9 0.4 all-to-all-done.1
  108.4 2.3 bitcast_subtract_fusion
  110.6 0.1 copy.135
  110.8 0.2 fusion.66
  111.0 0.1 copy.123
  111.1 0.7 copy.119
  111.9 0.6 copy.121
  112.5 0.6 fusion.65
  113.1 16.3 %all-gather.10.cloned.1.call-done = bf16[4,2048,128]{2,1,0:T(8,128)(2,1)} async-done(((bf16[4,512,128]{2,1,0:T(8,128)(2,1)}), bf16[4,2048,128]{2,1,0:T(8,128)(2,1)}) %all-gather.10.cloned.1.call-update) | async-done | bytes 2097168 | tf_op jit(solution)/shard_map/all_gather | solution.py:371
  129.4 4.2 %copy.133 = bf16[512,4,4,128]{0,3,2,1:T(8,128)(2,1)} copy(bf16[512,4,4,128]{3,0,2,1:T(8,128)(2,1)} %bitcast.145) | data formatting | bytes 4194304 | tf_op jit(solution)/shard_map/transpose | solution.py:426
  133.6 67.5 %all-gather.8.cloned.1.call-done = bf16[4,512,1536]{1,2,0:T(8,128)(2,1)} async-done(((bf16[4,128,1536]{1,2,0:T(8,128)(2,1)}), bf16[4,512,1536]{1,2,0:T(8,128)(2,1)}) %all-gather.8.cloned.1.call-update) | async-done | bytes 6291472 | tf_op jit(solution)/shard_map/all_gather | solution.py:370
  201.1 8.6 %copy.116 = bf16[4,512,1536]{2,1,0:T(8,128)(2,1)} copy(bf16[4,512,1536]{1,2,0:T(8,128)(2,1)} %all-gather.8.cloned.1.call-done) | data formatting | bytes 12582912 | tf_op jit(solution)/shard_map/all_gather | solution.py:370
  209.8 6.8 %convolution_convert_fusion.1 = bf16[512,1536]{1,0:T(8,128)(2,1)S(1)} fusion(bf16[512,2048]{1,0:T(8,128)(2,1)} %all-gather.6.cloned.1.call-done, bf16[2048,1536]{1,0:T(8,128)(2,1)} %bitcast.142), kind=kOutput, calls=%fused_computation.6 | convolution fusion | flops 3222011904 | bytes 9961472 | tf_op jit(solution)/shard_map/dot_general | solution.py:373
  216.6 0.9 fusion.64
  217.6 0.2 multiply_convert_fusion.4
  217.8 0.2 multiply_convert_fusion.5
  218.0 0.9 fusion.67
  219.0 0.3 multiply_convert_fusion.3
  219.3 0.2 reshape.222
  219.6 0.3 copy.122
  219.8 0.5 convolution_bitcast_fusion.1
  220.4 3.2 %while.13 = (s32[]{:T(128)}, f32[1,4,64,128]{3,2,1,0:T(8,128)S(1)}, f32[4,1,4,64,128]{4,3,2,1,0:T(8,128)S(1)}, f32[4,1,4]{2,1,0:T(1,128)}, f32[4,1,4,64,128]{4,3,2,1,0:T(8,128)S(1)}, /*index=5*/s32[]{:T(128)}, s32[]{:T(128)}) while((s32[]{:T(128)}, f32[1,4,64,128]{3,2,1,0:T(8,128)S(1)}, f32[4,1,4,64,128]{4,3,2,1,0:T(8,128)S(1)}, ...), condition=%wide.region_3.4_spmd.clone, body=%wide.region_2.3_spmd.clone.sunk | while | flops 131075 | bytes 655508 | solution.py:94
  220.4 0.7 fusion.81
  221.1 0.1 bitcast_add_fusion.2
  221.3 0.7 fusion.81
  221.9 0.1 bitcast_add_fusion.2
  222.1 0.6 fusion.81
  222.7 0.1 bitcast_add_fusion.2
  222.8 0.6 fusion.81
  223.4 0.1 bitcast_add_fusion.2
  223.5 0.4 fusion.9
  224.0 1.3 fusion.8
  225.2 0.4 copy.136
  225.7 0.6 reshape.221
  226.3 0.2 multiply_reduce_fusion
  226.5 1.1 copy.137
  227.7 1.7 fusion.39
  229.4 5.5 %select_convert_fusion = bf16[2,512,512]{2,1,0:T(8,128)(2,1)S(1)} fusion(f32[2,512,512]{2,1,0:T(8,128)S(1)} %get-tuple-element.111, f32[2]{0:T(128)S(1)} %copy-done.17, pred[512,512]{1,0:T(8,128)(4,1)S(1)} %copy-done.7, u8[512,512]{1,0:T(8,128)(4,1)S(1)} %get-tuple-element.110), kind=kOutput, calls=%fused_computation.9 | convolution fusion | flops 3237740544 | bytes 3670024 | tf_op jit(solution)/shard_map/htr,rs->hts/dot_general | solution.py:316
  234.9 0.5 convolution_convert_fusion.2
  235.4 0.1 copy.138
  235.5 0.2 multiply_convert_fusion.2
  235.7 4.2 %convolution_convert_fusion = bf16[512,2048]{1,0:T(8,128)(2,1)} fusion(bf16[512,2048]{0,1:T(8,128)(2,1)} %bitcast.146, bf16[512,256]{1,0:T(8,128)(2,1)S(1)} %copy.138, bf16[512,256]{1,0:T(8,128)(2,1)S(1)} %multiply_convert_fusion.2), kind=kOutput, calls=%fused_computation.5 | convolution fusion | flops 1075838976 | bytes 4718592 | tf_op jit(solution)/shard_map/dot_general | solution.py:427
  240.0 36.2 %reduce-scatter.2.cloned.1.call-done = bf16[64,2048]{1,0:T(8,128)(2,1)} async-done(((bf16[512,2048]{1,0:T(8,128)(2,1)}), bf16[64,2048]{1,0:T(8,128)(2,1)}) %reduce-scatter.2.cloned.1.call-update) | async-done | bytes 262160 | tf_op jit(solution)/shard_map/reduce_scatter | solution.py:428
  (67 shorter events, 0.9 us)
Async XLA Ops:
  6.5 101.8 %copy-start = (bf16[2048,32]{0,1:T(8,128)(2,1)S(1)}, bf16[2048,32]{0,1:T(8,128)(2,1)}, u32[]{:S(2)}) copy-start(bf16[2048,32]{0,1:T(8,128)(2,1)} %param.25) | copy-start | bytes 393220
  6.5 3.5 %copy-start.10 = (bf16[1024,128]{1,0:T(8,128)(2,1)S(1)}, bf16[1024,128]{1,0:T(8,128)(2,1)}, u32[]{:S(2)}) copy-start(bf16[1024,128]{1,0:T(8,128)(2,1)} %param.34) | copy-start | bytes 786436
  6.5 3.5 %copy-start.9 = (bf16[1024,128]{1,0:T(8,128)(2,1)S(1)}, bf16[1024,128]{1,0:T(8,128)(2,1)}, u32[]{:S(2)}) copy-start(bf16[1024,128]{1,0:T(8,128)(2,1)} %param.35) | copy-start | bytes 786436
  6.5 10.8 %copy-start.2 = (bf16[128,1024]{1,0:T(8,128)(2,1)S(1)}, bf16[128,1024]{1,0:T(8,128)(2,1)}, u32[]{:S(2)}) copy-start(bf16[128,1024]{1,0:T(8,128)(2,1)} %param.21) | copy-start | bytes 786436
  6.5 101.8 %all-gather.6.cloned.1.call-start = ((), (), s32[]{:S(2)}) async-start(), calls=%async_computation.4 | async-start | bytes 2621440 | tf_op jit(solution)/shard_map/all_gather | solution.py:362
  7.9 9.7 %copy-start.3 = (bf16[128,1024]{1,0:T(8,128)(2,1)S(1)}, bf16[128,1024]{1,0:T(8,128)(2,1)}, u32[]{:S(2)}) copy-start(bf16[128,1024]{1,0:T(8,128)(2,1)} %param.22) | copy-start | bytes 786436
  10.0 7.7 %copy-start.11 = (bf16[128,512]{1,0:T(8,128)(2,1)S(1)}, bf16[128,512]{1,0:T(8,128)(2,1)}, u32[]{:S(2)}) copy-start(bf16[128,512]{1,0:T(8,128)(2,1)} %param.23) | copy-start | bytes 393220
  10.0 7.9 %copy-start.12 = (bf16[128,512]{1,0:T(8,128)(2,1)S(1)}, bf16[128,512]{1,0:T(8,128)(2,1)}, u32[]{:S(2)}) copy-start(bf16[128,512]{1,0:T(8,128)(2,1)} %param.24) | copy-start | bytes 393220
  10.0 8.0 %copy-start.4 = (bf16[128,1024]{1,0:T(8,128)(2,1)S(1)}, bf16[128,1024]{1,0:T(8,128)(2,1)}, u32[]{:S(2)}) copy-start(bf16[128,1024]{1,0:T(8,128)(2,1)} %param.30) | copy-start | bytes 786436
  10.1 8.1 %copy-start.5 = (bf16[128,1024]{1,0:T(8,128)(2,1)S(1)}, bf16[128,1024]{1,0:T(8,128)(2,1)}, u32[]{:S(2)}) copy-start(bf16[128,1024]{1,0:T(8,128)(2,1)} %param.31) | copy-start | bytes 786436
  10.9 7.5 %copy-start.6 = (bf16[128,1024]{1,0:T(8,128)(2,1)S(1)}, bf16[128,1024]{1,0:T(8,128)(2,1)}, u32[]{:S(2)}) copy-start(bf16[128,1024]{1,0:T(8,128)(2,1)} %param.32) | copy-start | bytes 786436
  10.9 33.1 %all-to-all-start.2 = ((bf16[4,512,128]{2,1,0:T(8,128)(2,1)}), bf16[4,512,128]{2,1,0:T(8,128)(2,1)S(1)}, u32[]{:S(2)}, u32[]{:S(2)}) async-start(bf16[4,512,128]{2,1,0:T(8,128)(2,1)} %pad_maximum_fusion), calls=%async_computation.2 | async-start | bytes 1048576 | tf_op jit(solution)/shard_map/all_to_all | solution.py:369
  17.4 112.0 %all-gather.10.cloned.1.call-start = ((), (), s32[]{:S(2)}) async-start(), calls=%async_computation.7 | async-start | bytes 2621440 | tf_op jit(solution)/shard_map/all_gather | solution.py:371
  44.0 0.8 copy-start.1
  44.8 156.3 %all-gather.8.cloned.1.call-start = ((), (), s32[]{:S(2)}) async-start(), calls=%async_computation.6 | async-start | bytes 7864320 | tf_op jit(solution)/shard_map/all_gather | solution.py:370
  45.1 60.8 %copy-start.15 = (f32[32]{0:T(128)S(1)}, f32[32]{0:T(128)}, u32[]{:S(2)}) copy-start(f32[32]{0:T(128)} %param.27) | copy-start | bytes 388
  45.2 62.1 %copy-start.16 = (f32[16]{0:T(128)S(1)}, f32[16]{0:T(128)}, u32[]{:S(2)}) copy-start(f32[16]{0:T(128)} %param.33) | copy-start | bytes 196
  99.5 8.8 %all-to-all-start.1 = ((f32[128,4,4]{0,2,1:T(4,128)}), f32[128,4,4]{0,2,1:T(4,128)S(1)}, u32[]{:S(2)}, u32[]{:S(2)}) async-start(f32[128,4,4]{0,2,1:T(4,128)} %bitcast.25), calls=%async_computation.1 | async-start | bytes 16384 | tf_op jit(solution)/shard_map/all_to_all | solution.py:363
  102.8 173.4 %reduce-scatter.2.cloned.1.call-start = ((), (), s32[]{:S(2)}) async-start(), calls=%async_computation.5 | async-start | bytes 2359296 | tf_op jit(solution)/shard_map/reduce_scatter | solution.py:428
  220.4 3.6 %copy-start.8 = (f32[4,128,128]{2,1,0:T(8,128)S(1)}, f32[4,128,128]{2,1,0:T(8,128)}, u32[]{:S(2)}) copy-start(f32[4,128,128]{2,1,0:T(8,128)} %fusion.67) | copy-start | bytes 786436
  220.4 3.6 %copy-start.13 = (f32[4,4,128]{2,1,0:T(4,128)S(1)}, f32[4,4,128]{2,1,0:T(4,128)}, u32[]{:S(2)}) copy-start(f32[4,4,128]{2,1,0:T(4,128)} %copy.119) | copy-start | bytes 24580
  225.2 2.4 copy-start.17
  226.5 2.9 %copy-start.7 = (pred[512,512]{1,0:T(8,128)(4,1)S(1)}, pred[512,512]{1,0:T(8,128)(4,1)}, u32[]{:S(2)}) copy-start(pred[512,512]{1,0:T(8,128)(4,1)} %iota_compare_fusion.1) | copy-start | bytes 786436
  234.9 0.7 copy-start.14
Sparse Core Ops, SparseCore 0:
  10.2 82.6 all-gather.5
  94.7 34.6 all-gather.9
  131.2 69.8 all-gather.7
  240.1 36.0 reduce-scatter.1

commit v2 on v1

--- a/solution.py
+++ b/solution.py
@@ -1,6 +1,10 @@
+import functools
+
 import jax
 import jax.numpy as jnp
 from jax import lax
+from jax.experimental import pallas as pl
+from jax.experimental.pallas import tpu as pltpu
 from jax.sharding import PartitionSpec as P
 
 HEAD_DIM = 64
@@ -300,6 +304,323 @@
     return mixed[None]
 
 
+MESH = pl.DeviceIdType.MESH
+
+
+def remote(src, dst, send, recv, **where):
+    return pltpu.make_async_remote_copy(
+        src_ref=src,
+        dst_ref=dst,
+        send_sem=send,
+        recv_sem=recv,
+        device_id=where,
+        device_id_type=MESH,
+    )
+
+
+def greet(seq_count, fs_peers):
+    barrier = pltpu.get_barrier_semaphore()
+    s = lax.axis_index("sp")
+    peers = [{"tp": 1 - lax.axis_index("tp")}]
+    peers += [{"sp": lax.rem(s + d, seq_count)} for d in range(1, seq_count)]
+    peers += [{"fs": peer} for peer in fs_peers]
+    for peer in peers:
+        pl.semaphore_signal(barrier, inc=1, device_id=peer, device_id_type=MESH)
+    pl.semaphore_wait(barrier, len(peers))
+
+
+def gather_kernel(
+    seq_count,
+    batch_count,
+    gate,
+    inp,
+    bkey,
+    cquery,
+    query,
+    key,
+    value,
+    mixer,
+    attend,
+    normed,
+    offset,
+    mix_rows,
+    stick_rows,
+    out_rows,
+    all_normed,
+    all_offset,
+    own_sem,
+    z_send,
+    z_recv,
+    f_send,
+    f_recv,
+    h_send,
+    h_recv,
+    n_send,
+    n_recv,
+    p_send,
+    p_recv,
+    o_send,
+    o_recv,
+    last_sem,
+):
+    s, f, t = lax.axis_index("sp"), lax.axis_index("fs"), lax.axis_index("tp")
+    row_x = lax.rem(f, 2)
+    across = f + 1 - 2 * row_x
+    along = lax.rem(f + 2, 4)
+    greet(seq_count, (across, along))
+    depth = gate.shape[0]
+    piece_cols = out_rows.shape[1] // (seq_count * batch_count)
+    half_rows = normed.shape[0] // 2
+
+    def column_pieces(arrays):
+        found, at = [], 0
+        for ref in arrays:
+            found.append((ref, at, ref.shape[1] // seq_count))
+            at += found[-1][2]
+        return found
+
+    def row_pieces(arrays):
+        found, at = [], 0
+        for ref in arrays:
+            found.append((ref, at, ref.shape[0] // seq_count))
+            at += found[-1][2]
+        return found
+
+    kinds = (
+        (mix_rows, column_pieces((gate, inp, bkey, cquery)), False),
+        (stick_rows, column_pieces((query, key, value)), False),
+        (out_rows, row_pieces((mixer, attend)), True),
+    )
+
+    def chunk(kind, from_s, from_f):
+        dest, _, by_rows = kinds[kind]
+        if by_rows:
+            at = pl.multiple_of((from_s * batch_count + from_f) * piece_cols, piece_cols)
+            return dest.at[:, pl.ds(at, piece_cols)]
+        return dest.at[from_s, from_f]
+
+    def half(kind, from_s, from_f, which):
+        dest, _, by_rows = kinds[kind]
+        if by_rows:
+            rows = dest.shape[0] // 2
+            at = pl.multiple_of((from_s * batch_count + from_f) * piece_cols, piece_cols)
+            return dest.at[pl.ds(which * rows, rows), pl.ds(at, piece_cols)]
+        rows = depth // 2
+        return dest.at[from_s, from_f, pl.ds(which * rows, rows)]
+
+    def piece(kind, number, to_s, from_s):
+        dest, found, by_rows = kinds[kind]
+        ref, at, size = found[number]
+        start = pl.multiple_of(to_s * size, size)
+        if by_rows:
+            column = pl.multiple_of((from_s * batch_count + f) * piece_cols, piece_cols)
+            return (
+                ref.at[pl.ds(start, size), :],
+                dest.at[pl.ds(at, size), pl.ds(column, piece_cols)],
+            )
+        return ref.at[:, pl.ds(start, size)], dest.at[from_s, f, :, pl.ds(at, size)]
+
+    base = []
+    total = 0
+    for kind in range(3):
+        base.append(total)
+        total += len(kinds[kind][1])
+    sent = []
+
+    def begin(copy):
+        copy.start()
+        sent.append(copy)
+
+    own = [[] for _ in range(3)]
+    for kind in range(3):
+        for number in range(len(kinds[kind][1])):
+            source, dest = piece(kind, number, s, s)
+            copy = pltpu.make_async_copy(source, dest, own_sem.at[base[kind] + number])
+            copy.start()
+            own[kind].append(copy)
+    keep_normed = pltpu.make_async_copy(normed, all_normed.at[s], last_sem.at[0])
+    keep_normed.start()
+    keep_offset = pltpu.make_async_copy(offset.at[s], all_offset.at[s], last_sem.at[1])
+    keep_offset.start()
+
+    def send_kind(kind):
+        for d in range(1, seq_count):
+            q = lax.rem(s + d, seq_count)
+            for number in range(len(kinds[kind][1])):
+                source, dest = piece(kind, number, q, s)
+                at = base[kind] + number
+                begin(remote(source, dest, z_send.at[at, d], z_recv.at[at, d], sp=q))
+
+    def rows_of(from_s, which):
+        return all_normed.at[from_s, pl.ds(pl.multiple_of(which * half_rows, half_rows), half_rows)]
+
+    send_kind(0)
+    for d in range(1, seq_count):
+        q = lax.rem(s + d, seq_count)
+        source = normed.at[pl.ds(pl.multiple_of(t * half_rows, half_rows), half_rows)]
+        begin(remote(source, rows_of(s, t), n_send.at[d], n_recv.at[d], sp=q))
+        begin(remote(offset.at[q], all_offset.at[s], o_send.at[d], o_recv.at[d], sp=q))
+    send_kind(1)
+    send_kind(2)
+
+    def from_of(d):
+        return lax.rem(s + seq_count - d, seq_count)
+
+    def spread(kind, d):
+        from_s = from_of(d)
+        if d == 0:
+            for copy in own[kind]:
+                copy.wait()
+        else:
+            for number in range(len(kinds[kind][1])):
+                source, dest = piece(kind, number, s, from_s)
+                at = base[kind] + number
+                remote(source, dest, z_send.at[at, d], z_recv.at[at, d], sp=s).wait_recv()
+        block = chunk(kind, from_s, f)
+        begin(
+            remote(block, block, f_send.at[kind, d, 0], f_recv.at[kind, d, 0], fs=across)
+        )
+        begin(
+            remote(block, block, f_send.at[kind, d, 1], f_recv.at[kind, d, 1], fs=along)
+        )
+
+    def forward(kind, d):
+        from_s = from_of(d)
+        for which, (origin, target) in enumerate(((across, along), (along, across))):
+            block = chunk(kind, from_s, origin)
+            remote(
+                block, block, f_send.at[kind, d, which], f_recv.at[kind, d, which], fs=origin
+            ).wait_recv()
+            part = half(kind, from_s, origin, which)
+            begin(
+                remote(
+                    part, part, h_send.at[kind, d, which], h_recv.at[kind, d, which], fs=target
+                )
+            )
+
+    def arrive(kind):
+        opposite = 3 - f
+        for d in range(seq_count):
+            for which in range(2):
+                part = half(kind, from_of(d), opposite, which)
+                remote(
+                    part, part, h_send.at[kind, d, which], h_recv.at[kind, d, which], fs=across
+                ).wait_recv()
+
+    def share_normed():
+        for d in range(1, seq_count):
+            block = rows_of(from_of(d), t)
+            remote(block, block, n_send.at[d], n_recv.at[d], sp=s).wait_recv()
+            begin(remote(block, block, p_send.at[d], p_recv.at[d], tp=1 - t))
+
+    before = None
+    for kind in range(3):
+        for d in range(seq_count):
+            spread(kind, d)
+            if before is not None:
+                forward(*before)
+            before = (kind, d)
+        if kind == 0:
+            share_normed()
+    forward(*before)
+    for d in range(1, seq_count):
+        block = rows_of(from_of(d), 1 - t)
+        remote(block, block, p_send.at[d], p_recv.at[d], tp=1 - t).wait_recv()
+        remote(
+            offset.at[s], all_offset.at[from_of(d)], o_send.at[d], o_recv.at[d], sp=s
+        ).wait_recv()
+    keep_normed.wait()
+    keep_offset.wait()
+    for kind in range(3):
+        arrive(kind)
+    for copy in sent:
+        copy.wait_send()
+
+
+def gather_all(seq_count, batch_count, weights, outs, normed, offset):
+    depth = weights[0].shape[0]
+    mix = sum(w.shape[1] for w in weights[:4]) // seq_count
+    stick = sum(w.shape[1] for w in weights[4:]) // seq_count
+    rows = sum(w.shape[0] for w in outs) // seq_count
+    columns = outs[0].shape[1] * seq_count * batch_count
+    number = len(weights) + len(outs)
+    dma = pltpu.SemaphoreType.DMA
+    vmem = pl.BlockSpec(memory_space=pltpu.VMEM)
+    return pl.pallas_call(
+        functools.partial(gather_kernel, seq_count, batch_count),
+        out_shape=(
+            jax.ShapeDtypeStruct((seq_count, batch_count, depth, mix), jnp.bfloat16),
+            jax.ShapeDtypeStruct((seq_count, batch_count, depth, stick), jnp.bfloat16),
+            jax.ShapeDtypeStruct((rows, columns), jnp.bfloat16),
+            jax.ShapeDtypeStruct((seq_count,) + normed.shape, jnp.bfloat16),
+            jax.ShapeDtypeStruct(offset.shape, jnp.float32),
+        ),
+        in_specs=[pl.BlockSpec(memory_space=pltpu.HBM)] * (number + 2),
+        out_specs=(vmem,) * 5,
+        scratch_shapes=[
+            dma((number,)),
+            dma((number, seq_count)),
+            dma((number, seq_count)),
+            dma((3, seq_count, 2)),
+            dma((3, seq_count, 2)),
+            dma((3, seq_count, 2)),
+            dma((3, seq_count, 2)),
+            dma((seq_count,)),
+            dma((seq_count,)),
+            dma((seq_count,)),
+            dma((seq_count,)),
+            dma((seq_count,)),
+            dma((seq_count,)),
+            dma((2,)),
+        ],
+        compiler_params=pltpu.CompilerParams(collective_id=0, has_side_effects=True),
+    )(*weights, *outs, normed, offset)
+
+
+def scatter_kernel(seq_count, share, out, pair, joined, land, p_send, p_recv, z_send, z_recv):
+    s, t = lax.axis_index("sp"), lax.axis_index("tp")
+    greet(seq_count, ())
+    order = list(range(1, seq_count)) + [0]
+    sent = []
+    for d in order:
+        q = lax.rem(s + d, seq_count)
+        copy = remote(share.at[q, 1 - t], pair.at[d], p_send.at[d], p_recv.at[d], tp=1 - t)
+        copy.start()
+        sent.append(copy)
+    for number, d in enumerate(order):
+        q = lax.rem(s + d, seq_count)
+        sent[number].wait_recv()
+        joined[d] = (share[q, t].astype(jnp.float32) + pair[d].astype(jnp.float32)).astype(
+            jnp.bfloat16
+        )
+        if d:
+            copy = remote(joined.at[d], land.at[d], z_send.at[d], z_recv.at[d], sp=q)
+            copy.start()
+            sent.append(copy)
+    total = joined[0].astype(jnp.float32)
+    for d in range(1, seq_count):
+        remote(joined.at[d], land.at[d], z_send.at[d], z_recv.at[d], sp=s).wait_recv()
+        total = total + land[d].astype(jnp.float32)
+    out[...] = total.astype(jnp.bfloat16)
+    for copy in sent:
+        copy.wait_send()
+
+
+def scatter_sum(seq_count, share):
+    block = share.shape[2:]
+    vmem = pl.BlockSpec(memory_space=pltpu.VMEM)
+    dma = pltpu.SemaphoreType.DMA
+    return pl.pallas_call(
+        functools.partial(scatter_kernel, seq_count),
+        out_shape=jax.ShapeDtypeStruct(block, jnp.bfloat16),
+        in_specs=[vmem],
+        out_specs=vmem,
+        scratch_shapes=[pltpu.VMEM((seq_count,) + block, jnp.bfloat16)] * 3
+        + [dma((seq_count,))] * 4,
+        compiler_params=pltpu.CompilerParams(collective_id=1, has_side_effects=True),
+    )(share)
+
+
 def stick_heads(query_heads, key_heads, value_heads, bias_heads):
     length = query_heads.shape[0]
     logits = (
@@ -352,25 +673,23 @@
         widened * lax.rsqrt(jnp.mean(widened * widened, axis=-1, keepdims=True) + EPS) * norm_gain
     ).astype(jnp.bfloat16)
     weights = (w_gate, w_input, w_bkey, w_cquery, w_query, w_key, w_value)
-    depth = w_gate.shape[0]
     widths = [w.shape[1] // seq_count for w in weights]
-    packed = jnp.concatenate([w.reshape(depth, seq_count, -1) for w in weights], axis=2)
-    packed = jnp.transpose(packed, (1, 0, 2))
-    packed_out = jnp.concatenate(
-        [w.reshape(seq_count, -1, w.shape[1]) for w in (out_mixer, out_attend)], axis=1
-    )
-    normed = lax.all_gather(normed, "sp", axis=0, tiled=True)
-    offset = lax.all_to_all(
-        decay_offset[0].reshape(row_count, seq_count, -1), "sp", 1, 0, tiled=True
-    )
-    length = normed.shape[0]
-    offset = offset.reshape(length, -1)
-    packed = lax.all_to_all(packed, "sp", 0, 0, tiled=True)
-    packed_out = lax.all_to_all(packed_out, "sp", 0, 0, tiled=True)
-    packed = lax.all_gather(packed, "fs", axis=1)
-    packed_out = lax.all_gather(packed_out, "fs", axis=1)
-    rows = packed.reshape(width, -1)
-    projected = jnp.dot(normed, rows, preferred_element_type=jnp.float32).astype(jnp.bfloat16)
+    offset = jnp.transpose(decay_offset[0]).reshape(seq_count, -1, row_count)
+    mix_rows, stick_rows, out_rows, normed, offset = gather_all(
+        seq_count, batch_count, weights, (out_mixer, out_attend), normed, offset
+    )
+    length = seq_count * row_count
+    normed = normed.reshape(length, width)
+    offset = jnp.transpose(offset, (0, 2, 1)).reshape(length, -1)
+    projected = jnp.concatenate(
+        [
+            jnp.dot(
+                normed, rows.reshape(width, -1), preferred_element_type=jnp.float32
+            ).astype(jnp.bfloat16)
+            for rows in (mix_rows, stick_rows)
+        ],
+        axis=1,
+    )
     acts = []
     start = 0
     for w in widths:
@@ -423,15 +742,16 @@
         bias_heads,
     ).reshape(length, heads_stick * SB_DIM)
     y_both = jnp.concatenate([y_mixer, y_attend], axis=1)
-    out_rows = jnp.transpose(packed_out, (2, 0, 1, 3)).reshape(y_both.shape[1], -1)
     share = jnp.dot(y_both, out_rows, preferred_element_type=jnp.float32).astype(jnp.bfloat16)
-    mixed = lax.psum_scatter(share, ("sp", "tp"), scatter_dimension=0, tiled=True)
-    return mixed[None]
+    tensor_count = lax.axis_size("tp")
+    share = share.reshape(seq_count, tensor_count, row_count // tensor_count, width)
+    return scatter_sum(seq_count, share)[None]
 
 
 def by_heads(mesh):
     groups = GROUP_WIDTH // STATE
-    return groups % (mesh.shape["tp"] * mesh.shape["sp"]) == 0
+    fits = groups % (mesh.shape["tp"] * mesh.shape["sp"]) == 0
+    return fits and mesh.shape["tp"] == 2 and mesh.shape["fs"] == 4
 
 
 def solution(mesh):

time: 284 us -> 178 us (0.63)
  the two profiles are of different devices: /device:TPU:0 before, /device:TPU:9 now
where the time goes in v2:
time: 178 us
  Pallas kernels  141 us (79%)
  matrix products  21.3 us (12%)
  local copies, waits for them, and re-layouts  9.71 us (5%)
  other arithmetic  5.34 us (3%)
    pallas_call x1, Pallas kernels, gather_all(): pl.pallas_call(functools.partial(gather_kernel, seq_count, batch_count),...  108 us
    pallas_call x1, Pallas kernels, scatter_sum(): pl.pallas_call(functools.partial(scatter_kernel, seq_count), out_shape=ja...  32.2 us
    dot_general x2, matrix products, head_body(): jnp.dot(normed, rows.reshape(width, -1), preferred_element_type=jnp.float32)  8.01 us
    dot_general x1, matrix products, stick_heads(): jnp.einsum('htr,rs->hts', log_pass, later, precision=lax.Precision.HIGHEST)  5.65 us
    dot_general x1, matrix products, head_body(): jnp.dot(y_both, out_rows, preferred_element_type=jnp.float32)  4.21 us

profile of v2, /device:TPU:9, one launch (start us, length us, event | category | flops | bytes accessed | tf_op | source)
XLA Modules:
  0.0 177.5 jit_solution(12218263864965505143)
XLA Ops:
  0.0 0.0 copy-start
  0.0 1.3 fusion.10
  1.3 2.0 %fusion.12.normed = bf16[128,2048]{1,0:T(8,128)(2,1)} fusion(bf16[1,128,2048]{2,1,0:T(8,128)(2,1)} %param.19, f32[2048]{0:T(1024)} %param.20, f32[128]{0:T(128)S(1)} %add_rsqrt_fusion.1), kind=kLoop, calls=%fused_computation.27 | loop fusion | flops 1048576 | bytes 1057280 | tf_op jit(solution)/shard_map/convert_element_type | solution.py:674
  3.3 108.4 %shard_map.163 = (bf16[4,4,128,768]{3,2,1,0:T(8,128)(2,1)}, bf16[4,4,128,768]{3,2,1,0:T(8,128)(2,1)}, bf16[512,2048]{1,0:T(8,128)(2,1)}, bf16[4,128,2048]{2,1,0:T(8,128)(2,1)}, f32[4,4,128]{2,1,0:T(4,128)}) custom-call(bf16[128,1024]{1,0:T(8,128)(2,1)} %gate.1, bf16[128,1024]{1,0:T(8,128)(2,1)} %inp.1, bf16[128,512]{1,0:T(8,128)(2,1)} %bkey.1, ...), custom_call_target="tpu_custom_call" | custom-call | tf_op jit(solution)/shard_map/pallas_call | solution.py:549
  111.7 4.3 %convolution_convert_fusion.1 = bf16[512,768]{1,0:T(8,128)(2,1)S(1)} fusion(bf16[512,2048]{1,0:T(8,128)(2,1)} %bitcast.137, bf16[2048,768]{1,0:T(8,128)(2,1)} %bitcast.156), kind=kOutput, calls=%fused_computation.15 | convolution fusion | flops 1611005952 | bytes 6029312 | tf_op jit(solution)/shard_map/dot_general | solution.py:686
  116.0 0.0 copy-start.11
  116.0 0.1 slice_bitcast_fusion.1
  116.1 0.1 copy.71
  116.3 0.4 copy-done.11
  116.7 0.1 dynamic_slice.35
  116.7 0.7 fusion.39
  117.4 0.1 iota_compare_fusion.1
  117.5 5.7 %select_convert_fusion = bf16[2,512,512]{2,1,0:T(8,128)(2,1)S(1)} fusion(f32[2,512,512]{2,1,0:T(8,128)S(1)} %get-tuple-element.110, f32[2]{0:T(128)S(1)} %dynamic_slice.35, pred[512,512]{1,0:T(8,128)(4,1)S(1)} %iota_compare_fusion.1, u8[512,512]{1,0:T(8,128)(4,1)S(1)} %get-tuple-element.109), kind=kOutput, calls=%fused_computation.8 | convolution fusion | flops 3237740544 | bytes 3670024 | tf_op jit(solution)/shard_map/htr,rs->hts/dot_general | solution.py:637
  123.2 0.0 copy-start.1
  123.2 0.5 convolution_convert_fusion.3
  123.6 0.1 copy.72
  123.8 1.3 dynamic_slice.34
  125.1 0.0 copy-done.1
  125.1 3.7 %convolution_convert_fusion.2 = bf16[512,768]{1,0:T(8,128)(2,1)S(1)} fusion(bf16[512,2048]{1,0:T(8,128)(2,1)S(1)} %bitcast.138, bf16[2048,768]{1,0:T(8,128)(2,1)} %bitcast.155), kind=kOutput, calls=%fused_computation.16 | convolution fusion | flops 1611005952 | bytes 6029312 | tf_op jit(solution)/shard_map/dot_general | solution.py:686
  128.8 0.0 copy-start.2
  128.8 0.0 copy-start.5
  128.9 0.9 copy-done.2
  129.7 0.1 pad_convert_fusion.1
  129.8 0.7 constant_dynamic-slice_fusion.2
  130.5 0.5 slice_bitcast_fusion.5
  131.0 0.2 multiply_convert_fusion.5
  131.2 0.7 dynamic_slice.32
  132.0 0.0 copy-done
  132.0 0.0 copy-done.5
  132.0 0.7 bitcast_subtract_fusion
  132.7 0.1 copy.69
  132.8 0.2 fusion.65
  133.0 0.1 pad_convert_fusion
  133.1 0.9 constant_dynamic-slice_fusion.1
  134.0 0.0 copy-start.9
  134.0 0.0 copy-start.10
  134.0 0.3 multiply_convert_fusion.3
  134.4 0.2 reshape.194
  134.6 0.3 copy.57
  134.9 0.1 copy.58
  135.0 0.1 bitcast_exponential_fusion
  135.1 0.0 copy-done.7
  135.2 0.2 multiply_convert_fusion.4
  135.4 0.5 convolution_bitcast_fusion.1
  135.9 0.0 copy-done.4
  135.9 0.6 while.13
  136.0 0.1 bitcast_add_fusion.2
  136.1 0.1 bitcast_add_fusion.2
  136.3 0.1 bitcast_add_fusion.2
  136.4 0.1 bitcast_add_fusion.2
  136.5 0.4 fusion.9
  136.9 0.1 copy.54
  137.0 0.2 fusion.66
  137.3 0.5 fusion.8
  137.8 0.0 copy-start.3
  137.8 0.0 copy-start.6
  137.8 0.4 copy.70
  138.3 0.6 reshape.193
  138.9 0.1 copy-done.3
  139.0 0.2 multiply_reduce_fusion
  139.2 0.2 multiply_convert_fusion.2
  139.4 4.2 %convolution_convert_fusion = bf16[512,2048]{1,0:T(8,128)(2,1)} fusion(bf16[512,2048]{1,0:T(8,128)(2,1)} %get-tuple-element.42, bf16[512,256]{1,0:T(8,128)(2,1)S(1)} %copy.72, bf16[512,256]{1,0:T(8,128)(2,1)S(1)} %multiply_convert_fusion.2), kind=kOutput, calls=%fused_computation.5 | convolution fusion | flops 1075838976 | bytes 4718592 | tf_op jit(solution)/shard_map/dot_general | solution.py:745
  143.6 32.2 %shard_map.164 = bf16[64,2048]{1,0:T(8,128)(2,1)} custom-call(bf16[4,2,64,2048]{3,2,1,0:T(8,128)(2,1)} %bitcast.136), custom_call_target="tpu_custom_call" | custom-call | tf_op jit(solution)/shard_map/pallas_call | solution.py:613
  175.9 1.7 copy.101
  (27 shorter events, 0.2 us)
Async XLA Ops:
  0.0 132.0 %copy-start = (bf16[2048,32]{0,1:T(8,128)(2,1)S(1)}, bf16[2048,32]{0,1:T(8,128)(2,1)}, u32[]{:S(2)}) copy-start(bf16[2048,32]{0,1:T(8,128)(2,1)} %param.25) | copy-start | bytes 393220
  116.0 0.7 copy-start.11
  123.2 2.0 %copy-start.1 = (bf16[4,128,2048]{2,1,0:T(8,128)(2,1)S(1)}, bf16[4,128,2048]{2,1,0:T(8,128)(2,1)}, u32[]{:S(2)}) copy-start(bf16[4,128,2048]{2,1,0:T(8,128)(2,1)} %get-tuple-element.37) | copy-start | bytes 6291460
  128.8 0.9 copy-start.2
  128.8 3.1 %copy-start.5 = (f32[4,4,128]{2,1,0:T(4,128)S(1)}, f32[4,4,128]{2,1,0:T(4,128)}, u32[]{:S(2)}) copy-start(f32[4,4,128]{2,1,0:T(4,128)} %get-tuple-element.39) | copy-start | bytes 24580
  131.0 2.0 %slice-start = ((bf16[512,768]{1,0:T(8,128)(2,1)}), bf16[512,256]{1,0:T(8,128)(2,1)S(1)}, s32[]{:S(2)}) async-start(bf16[512,768]{1,0:T(8,128)(2,1)} %copy-done.2), calls=%async_computation | async-start | bytes 524288 | tf_op jit(solution)/shard_map/slice | solution.py:696
  134.0 1.1 copy-start.7
  134.0 1.1 copy-start.8
  134.0 1.1 copy-start.9
  134.0 1.1 copy-start.10
  134.4 1.5 copy-start.4
  137.8 1.1 copy-start.3
  137.8 1.4 copy-start.6

commit v3 on v2

--- a/solution.py
+++ b/solution.py
@@ -316,6 +316,19 @@
         device_id=where,
         device_id_type=MESH,
     )
+
+
+def partner(place, mask, count):
+    found, bit = 0, 1
+    while bit < count:
+        own = lax.rem(lax.div(place, bit), 2)
+        found = found + bit * (1 - own if mask & bit else own)
+        bit *= 2
+    return found
+
+
+def partner_order(count):
+    return list(range((count + 1) // 2, count)) + list(range(1, (count + 1) // 2))
 
 
 def greet(seq_count, fs_peers):
@@ -443,9 +456,11 @@
     keep_offset = pltpu.make_async_copy(offset.at[s], all_offset.at[s], last_sem.at[1])
     keep_offset.start()
 
+    order = partner_order(seq_count)
+
     def send_kind(kind):
-        for d in range(1, seq_count):
-            q = lax.rem(s + d, seq_count)
+        for d in order:
+            q = partner(s, d, seq_count)
             for number in range(len(kinds[kind][1])):
                 source, dest = piece(kind, number, q, s)
                 at = base[kind] + number
@@ -454,17 +469,16 @@
     def rows_of(from_s, which):
         return all_normed.at[from_s, pl.ds(pl.multiple_of(which * half_rows, half_rows), half_rows)]
 
-    send_kind(0)
-    for d in range(1, seq_count):
-        q = lax.rem(s + d, seq_count)
+    for kind in range(3):
+        send_kind(kind)
+    for d in order:
+        q = partner(s, d, seq_count)
         source = normed.at[pl.ds(pl.multiple_of(t * half_rows, half_rows), half_rows)]
         begin(remote(source, rows_of(s, t), n_send.at[d], n_recv.at[d], sp=q))
         begin(remote(offset.at[q], all_offset.at[s], o_send.at[d], o_recv.at[d], sp=q))
-    send_kind(1)
-    send_kind(2)
 
     def from_of(d):
-        return lax.rem(s + seq_count - d, seq_count)
+        return partner(s, d, seq_count)
 
     def spread(kind, d):
         from_s = from_of(d)
@@ -508,21 +522,21 @@
                 ).wait_recv()
 
     def share_normed():
-        for d in range(1, seq_count):
+        for d in order:
             block = rows_of(from_of(d), t)
             remote(block, block, n_send.at[d], n_recv.at[d], sp=s).wait_recv()
             begin(remote(block, block, p_send.at[d], p_recv.at[d], tp=1 - t))
 
     before = None
-    for kind in range(3):
-        for d in range(seq_count):
-            spread(kind, d)
-            if before is not None:
-                forward(*before)
-            before = (kind, d)
-        if kind == 0:
-            share_normed()
+    steps = [(kind, 0) for kind in range(3)]
+    steps += [(kind, d) for kind in range(3) for d in order]
+    for step in steps:
+        spread(*step)
+        if before is not None:
+            forward(*before)
+        before = step
     forward(*before)
+    share_normed()
     for d in range(1, seq_count):
         block = rows_of(from_of(d), 1 - t)
         remote(block, block, p_send.at[d], p_recv.at[d], tp=1 - t).wait_recv()
@@ -577,22 +591,39 @@
     )(*weights, *outs, normed, offset)
 
 
-def scatter_kernel(seq_count, share, out, pair, joined, land, p_send, p_recv, z_send, z_recv):
+def scatter_kernel(
+    seq_count,
+    mixer,
+    attend,
+    rows,
+    out,
+    share,
+    pair,
+    joined,
+    land,
+    p_send,
+    p_recv,
+    z_send,
+    z_recv,
+):
     s, t = lax.axis_index("sp"), lax.axis_index("tp")
     greet(seq_count, ())
-    order = list(range(1, seq_count)) + [0]
+    order = partner_order(seq_count) + [0]
+    width = mixer.shape[2]
     sent = []
     for d in order:
-        q = lax.rem(s + d, seq_count)
-        copy = remote(share.at[q, 1 - t], pair.at[d], p_send.at[d], p_recv.at[d], tp=1 - t)
+        q = partner(s, d, seq_count)
+        summed = jnp.dot(mixer[q], rows[:width], preferred_element_type=jnp.float32)
+        summed += jnp.dot(attend[q], rows[width:], preferred_element_type=jnp.float32)
+        share[d] = summed.astype(jnp.bfloat16).reshape(share.shape[1:])
+        copy = remote(share.at[d, 1 - t], pair.at[d], p_send.at[d], p_recv.at[d], tp=1 - t)
         copy.start()
         sent.append(copy)
     for number, d in enumerate(order):
-        q = lax.rem(s + d, seq_count)
+        q = partner(s, d, seq_count)
         sent[number].wait_recv()
-        joined[d] = (share[q, t].astype(jnp.float32) + pair[d].astype(jnp.float32)).astype(
-            jnp.bfloat16
-        )
+        both = share[d, t].astype(jnp.float32) + pair[d].astype(jnp.float32)
+        joined[d] = both.astype(jnp.bfloat16)
         if d:
             copy = remote(joined.at[d], land.at[d], z_send.at[d], z_recv.at[d], sp=q)
             copy.start()
@@ -606,19 +637,20 @@
         copy.wait_send()
 
 
-def scatter_sum(seq_count, share):
-    block = share.shape[2:]
+def scatter_sum(seq_count, tensor_count, mixer, attend, rows):
+    block = (mixer.shape[1] // tensor_count, rows.shape[1])
     vmem = pl.BlockSpec(memory_space=pltpu.VMEM)
     dma = pltpu.SemaphoreType.DMA
     return pl.pallas_call(
         functools.partial(scatter_kernel, seq_count),
         out_shape=jax.ShapeDtypeStruct(block, jnp.bfloat16),
-        in_specs=[vmem],
+        in_specs=[vmem] * 3,
         out_specs=vmem,
-        scratch_shapes=[pltpu.VMEM((seq_count,) + block, jnp.bfloat16)] * 3
+        scratch_shapes=[pltpu.VMEM((seq_count, tensor_count) + block, jnp.bfloat16)]
+        + [pltpu.VMEM((seq_count,) + block, jnp.bfloat16)] * 3
         + [dma((seq_count,))] * 4,
         compiler_params=pltpu.CompilerParams(collective_id=1, has_side_effects=True),
-    )(share)
+    )(mixer, attend, rows)
 
 
 def stick_heads(query_heads, key_heads, value_heads, bias_heads):
@@ -741,11 +773,13 @@
         value_act.reshape(length, heads_stick, SB_DIM),
         bias_heads,
     ).reshape(length, heads_stick * SB_DIM)
-    y_both = jnp.concatenate([y_mixer, y_attend], axis=1)
-    share = jnp.dot(y_both, out_rows, preferred_element_type=jnp.float32).astype(jnp.bfloat16)
-    tensor_count = lax.axis_size("tp")
-    share = share.reshape(seq_count, tensor_count, row_count // tensor_count, width)
-    return scatter_sum(seq_count, share)[None]
+    return scatter_sum(
+        seq_count,
+        lax.axis_size("tp"),
+        y_mixer.reshape(seq_count, row_count, -1),
+        y_attend.reshape(seq_count, row_count, -1),
+        out_rows,
+    )[None]
 
 
 def by_heads(mesh):

time: 178 us -> 160 us (0.90)
  Pallas kernels: 141 us -> 125 us
  matrix products: 21.3 us -> 16.9 us
  other arithmetic: 5.34 us -> 8.14 us
    pallas_call x1, Pallas kernels: 108 us -> 89.7 us  [gather_all(): pl.pallas_call(functools.partial(gather_kernel, seq_count, batch_count),...]
    dot_general x1 -> x0, matrix products: 4.21 us -> none  [head_body(): jnp.dot(y_both, out_rows, preferred_element_type=jnp.float32)]
    pallas_call x1, Pallas kernels: 32.2 us -> 34.9 us  [scatter_sum(): pl.pallas_call(functools.partial(scatter_kernel, seq_count), out_shape=ja...]
where the time goes in v3:
time: 160 us; the launch traced here: 159 us
  Pallas kernels  125 us (78%)
  matrix products  16.9 us (11%)
  local copies, waits for them, and re-layouts  8.65 us (5%)
  other arithmetic  8.14 us (5%)
    pallas_call x1, Pallas kernels, gather_all(): pl.pallas_call(functools.partial(gather_kernel, seq_count, batch_count),...  89.7 us
    pallas_call x1, Pallas kernels, scatter_sum(): pl.pallas_call(functools.partial(scatter_kernel, seq_count), out_shape=ja...  34.9 us
    dot_general x2, matrix products, head_body(): jnp.dot(normed, rows.reshape(width, -1), preferred_element_type=jnp.float32)  7.98 us
    dot_general x1, matrix products, stick_heads(): jnp.einsum('htr,rs->hts', log_pass, later, precision=lax.Precision.HIGHEST)  5.47 us

profile of v3, /device:TPU:9, one launch (start us, length us, event | category | flops | bytes accessed | tf_op | source)
XLA Modules:
  0.0 159.0 jit_solution(17236643556177940020)
XLA Ops:
  0.0 0.0 copy-start
  0.0 1.3 fusion.11
  1.3 2.1 %fusion.13.normed = bf16[128,2048]{1,0:T(8,128)(2,1)} fusion(bf16[1,128,2048]{2,1,0:T(8,128)(2,1)} %param.19, f32[2048]{0:T(1024)} %param.20, f32[128]{0:T(128)S(1)} %add_rsqrt_fusion.1), kind=kLoop, calls=%fused_computation.27 | loop fusion | flops 1048576 | bytes 1057280 | tf_op jit(solution)/shard_map/convert_element_type | solution.py:706
  3.3 89.7 %shard_map.163 = (bf16[4,4,128,768]{3,2,1,0:T(8,128)(2,1)}, bf16[4,4,128,768]{3,2,1,0:T(8,128)(2,1)}, bf16[512,2048]{1,0:T(8,128)(2,1)}, bf16[4,128,2048]{2,1,0:T(8,128)(2,1)}, f32[4,4,128]{2,1,0:T(4,128)}) custom-call(bf16[128,1024]{1,0:T(8,128)(2,1)} %gate.1, bf16[128,1024]{1,0:T(8,128)(2,1)} %inp.1, bf16[128,512]{1,0:T(8,128)(2,1)} %bkey.1, ...), custom_call_target="tpu_custom_call" | custom-call | tf_op jit(solution)/shard_map/pallas_call | solution.py:563
  93.0 4.3 %convolution_convert_fusion.1 = bf16[512,768]{1,0:T(8,128)(2,1)S(1)} fusion(bf16[512,2048]{1,0:T(8,128)(2,1)} %bitcast.137, bf16[2048,768]{1,0:T(8,128)(2,1)} %bitcast.155), kind=kOutput, calls=%fused_computation.15 | convolution fusion | flops 1611005952 | bytes 6029312 | tf_op jit(solution)/shard_map/dot_general | solution.py:718
  97.3 0.0 copy-start.3
  97.3 0.0 copy-start.6
  97.3 0.0 copy-start.1
  97.3 0.0 copy-start.5
  97.4 0.8 copy-done.3
  98.2 0.1 pad_convert_fusion.1
  98.3 0.7 constant_dynamic-slice_fusion.2
  99.0 0.2 multiply_convert_fusion.5
  99.2 0.0 copy-done.6
  99.2 0.1 dynamic_slice.32
  99.3 0.0 copy-done
  99.3 0.0 copy-done.1
  99.3 0.0 copy-done.5
  99.3 0.7 bitcast_subtract_fusion
  100.0 0.1 copy.69
  100.1 0.2 fusion.62
  100.3 0.0 slice-done
  100.3 0.1 pad_convert_fusion
  100.4 0.9 constant_dynamic-slice_fusion.1
  101.3 0.3 multiply_convert_fusion.3
  101.7 0.0 copy-start.4
  101.7 0.2 reshape.197
  101.9 0.3 copy.57
  102.2 0.1 copy.58
  102.3 0.1 bitcast_exponential_fusion
  102.4 0.2 multiply_convert_fusion.4
  102.6 0.5 convolution_bitcast_fusion.1
  103.1 0.0 copy-done.4
  103.2 0.8 while.13
  103.4 0.1 bitcast_add_fusion.2
  103.5 0.1 bitcast_add_fusion.2
  103.7 0.1 bitcast_add_fusion.2
  103.8 0.1 bitcast_add_fusion.2
  103.9 0.4 fusion.9
  104.3 0.1 copy.54
  104.4 0.2 fusion.63
  104.7 0.5 fusion.8
  105.2 0.4 copy.70
  105.7 0.6 reshape.195
  106.3 0.0 copy-start.2
  106.3 1.3 multiply_reduce_fusion
  107.6 1.1 broadcast_multiply_fusion
  108.8 0.8 dynamic_slice.34
  109.5 0.7 multiply_convert_fusion.2.mixer
  110.3 0.0 copy-done.2
  110.3 3.7 %convolution_convert_fusion = bf16[512,768]{1,0:T(8,128)(2,1)S(1)} fusion(bf16[512,2048]{1,0:T(8,128)(2,1)S(1)} %bitcast.139, bf16[2048,768]{1,0:T(8,128)(2,1)} %bitcast.154), kind=kOutput, calls=%fused_computation.14 | convolution fusion | flops 1611005952 | bytes 6029312 | tf_op jit(solution)/shard_map/dot_general | solution.py:718
  114.0 0.0 copy-start.7
  114.0 0.1 slice_bitcast_fusion.1
  114.1 0.1 copy.71
  114.2 0.4 copy-done.7
  114.6 0.1 dynamic_slice.35
  114.7 0.7 fusion.37
  115.4 0.1 iota_compare_fusion.1
  115.5 5.5 %select_convert_fusion = bf16[2,512,512]{2,1,0:T(8,128)(2,1)S(1)} fusion(f32[2,512,512]{2,1,0:T(8,128)S(1)} %get-tuple-element.112, f32[2]{0:T(128)S(1)} %dynamic_slice.35, pred[512,512]{1,0:T(8,128)(4,1)S(1)} %iota_compare_fusion.1, u8[512,512]{1,0:T(8,128)(4,1)S(1)} %get-tuple-element.111), kind=kOutput, calls=%fused_computation.7 | convolution fusion | flops 3237740544 | bytes 3670024 | tf_op jit(solution)/shard_map/htr,rs->hts/dot_general | solution.py:669
  120.9 0.5 fusion.10
  121.4 0.1 reshape.196
  121.5 0.9 copy.72.attend
  122.4 34.9 %shard_map.164 = bf16[64,2048]{1,0:T(8,128)(2,1)} custom-call(bf16[4,128,256]{2,1,0:T(8,128)(2,1)} %multiply_convert_fusion.2.mixer, bf16[4,128,256]{2,1,0:T(8,128)(2,1)} %copy.72.attend, bf16[512,2048]{1,0:T(8,128)(2,1)} %get-tuple-element.42.rows), custom_call_target="tpu_custom_call" | custom-call | tf_op jit(solution)/shard_map/pallas_call | solution.py:644
  157.3 1.7 %copy.101 = bf16[1,64,2048]{2,1,0:T(8,128)(2,1)} copy(bf16[1,64,2048]{2,1,0:T(8,128)(2,1)} %bitcast.146) | data formatting | bytes 524288
  (20 shorter events, 0.2 us)
Async XLA Ops:
  0.0 99.3 %copy-start = (bf16[2048,32]{0,1:T(8,128)(2,1)S(1)}, bf16[2048,32]{0,1:T(8,128)(2,1)}, u32[]{:S(2)}) copy-start(bf16[2048,32]{0,1:T(8,128)(2,1)} %param.25) | copy-start | bytes 393220
  97.3 0.9 copy-start.3
  97.3 1.9 %copy-start.6 = (f32[32]{0:T(128)S(1)}, f32[32]{0:T(128)}, u32[]{:S(2)}) copy-start(f32[32]{0:T(128)} %param.27) | copy-start | bytes 388
  97.3 1.9 %copy-start.1 = (bf16[4,128,2048]{2,1,0:T(8,128)(2,1)S(1)}, bf16[4,128,2048]{2,1,0:T(8,128)(2,1)}, u32[]{:S(2)}) copy-start(bf16[4,128,2048]{2,1,0:T(8,128)(2,1)} %get-tuple-element.37) | copy-start | bytes 6291460
  97.3 1.9 %copy-start.5 = (f32[4,4,128]{2,1,0:T(4,128)S(1)}, f32[4,4,128]{2,1,0:T(4,128)}, u32[]{:S(2)}) copy-start(f32[4,4,128]{2,1,0:T(4,128)} %get-tuple-element.39) | copy-start | bytes 24580
  99.0 1.4 slice-start
  101.7 1.5 copy-start.4
  106.3 4.0 %copy-start.2 = (bf16[4,128,2048]{2,1,0:T(8,128)(2,1)S(1)}, bf16[4,128,2048]{2,1,0:T(8,128)(2,1)}, u32[]{:S(2)}) copy-start(bf16[4,128,2048]{2,1,0:T(8,128)(2,1)} %get-tuple-element.37) | copy-start | bytes 6291460
  114.0 0.7 copy-start.7

commit v4 on v3

--- a/solution.py
+++ b/solution.py
@@ -474,7 +474,8 @@
     for d in order:
         q = partner(s, d, seq_count)
         source = normed.at[pl.ds(pl.multiple_of(t * half_rows, half_rows), half_rows)]
-        begin(remote(source, rows_of(s, t), n_send.at[d], n_recv.at[d], sp=q))
+        if d & (d - 1) == 0:
+            begin(remote(source, rows_of(s, t), n_send.at[d], n_recv.at[d], sp=q))
         begin(remote(offset.at[q], all_offset.at[s], o_send.at[d], o_recv.at[d], sp=q))
 
     def from_of(d):
@@ -522,9 +523,14 @@
                 ).wait_recv()
 
     def share_normed():
-        for d in order:
+        for d in sorted(order, key=lambda d: (d & (d - 1) != 0, -d)):
             block = rows_of(from_of(d), t)
             remote(block, block, n_send.at[d], n_recv.at[d], sp=s).wait_recv()
+            for bit in (1, 2):
+                if d > bit and d & (d - 1) == 0 and d + bit < seq_count:
+                    q = partner(s, bit, seq_count)
+                    at = d + bit
+                    begin(remote(block, block, n_send.at[at], n_recv.at[at], sp=q))
             begin(remote(block, block, p_send.at[d], p_recv.at[d], tp=1 - t))
 
     before = None
@@ -666,7 +672,7 @@
     log_keep = jax.nn.log_sigmoid(logits)
     log_pass = jnp.where(before, log_keep - logits, 0.0)
     later = (row_index > col_index).astype(jnp.float32)
-    tail_sum = jnp.einsum("htr,rs->hts", log_pass, later, precision=lax.Precision.HIGHEST)
+    tail_sum = jnp.einsum("htr,rs->hts", log_pass, later, precision=lax.Precision.HIGH)
     weights = jnp.where(before, jnp.exp(log_keep + tail_sum), 0.0)
     return jnp.einsum(
         "hts,shd->thd",
@@ -785,7 +791,7 @@
 def by_heads(mesh):
     groups = GROUP_WIDTH // STATE
     fits = groups % (mesh.shape["tp"] * mesh.shape["sp"]) == 0
-    return fits and mesh.shape["tp"] == 2 and mesh.shape["fs"] == 4
+    return fits and mesh.shape["tp"] == 2 and mesh.shape["fs"] == 4 and mesh.shape["sp"] <= 4
 
 
 def solution(mesh):

time: 160 us -> 156 us (0.975); the launches traced: 159 us -> 153 us
  Pallas kernels: 125 us -> 119 us
    pallas_call x1, Pallas kernels: 34.9 us -> 29.8 us  [scatter_sum(): pl.pallas_call(functools.partial(scatter_kernel, seq_count), out_shape=ja...]
where the time goes in v4:
time: 156 us; the launch traced here: 153 us
  Pallas kernels  119 us (76%)
  matrix products  16.2 us (10%)
  local copies, waits for them, and re-layouts  8.65 us (6%)
  other arithmetic  8.14 us (5%)
    pallas_call x1, Pallas kernels, gather_all(): pl.pallas_call(functools.partial(gather_kernel, seq_count, batch_count),...  89.3 us
    pallas_call x1, Pallas kernels, scatter_sum(): pl.pallas_call(functools.partial(scatter_kernel, seq_count), out_shape=ja...  29.8 us
    dot_general x2, matrix products, head_body(): jnp.dot(normed, rows.reshape(width, -1), preferred_element_type=jnp.float32)  7.98 us
    dot_general x1, matrix products, stick_heads(): jnp.einsum('htr,rs->hts', log_pass, later, precision=lax.Precision.HIGH)  4.74 us

profile of v4, /device:TPU:9, one launch (start us, length us, event | category | flops | bytes accessed | tf_op | source)
XLA Modules:
  0.0 152.8 jit_solution(2992150784134772489)
XLA Ops:
  0.0 0.0 copy-start
  0.0 1.3 fusion.11
  1.3 2.1 %fusion.13.normed = bf16[128,2048]{1,0:T(8,128)(2,1)} fusion(bf16[1,128,2048]{2,1,0:T(8,128)(2,1)} %param.19, f32[2048]{0:T(1024)} %param.20, f32[128]{0:T(128)S(1)} %add_rsqrt_fusion.1), kind=kLoop, calls=%fused_computation.27 | loop fusion | flops 1048576 | bytes 1057280 | tf_op jit(solution)/shard_map/convert_element_type | solution.py:712
  3.3 89.3 %shard_map.163 = (bf16[4,4,128,768]{3,2,1,0:T(8,128)(2,1)}, bf16[4,4,128,768]{3,2,1,0:T(8,128)(2,1)}, bf16[512,2048]{1,0:T(8,128)(2,1)}, bf16[4,128,2048]{2,1,0:T(8,128)(2,1)}, f32[4,4,128]{2,1,0:T(4,128)}) custom-call(bf16[128,1024]{1,0:T(8,128)(2,1)} %gate.1, bf16[128,1024]{1,0:T(8,128)(2,1)} %inp.1, bf16[128,512]{1,0:T(8,128)(2,1)} %bkey.1, ...), custom_call_target="tpu_custom_call" | custom-call | tf_op jit(solution)/shard_map/pallas_call | solution.py:569
  92.6 4.3 %convolution_convert_fusion.1 = bf16[512,768]{1,0:T(8,128)(2,1)S(1)} fusion(bf16[512,2048]{1,0:T(8,128)(2,1)} %bitcast.137, bf16[2048,768]{1,0:T(8,128)(2,1)} %bitcast.155), kind=kOutput, calls=%fused_computation.15 | convolution fusion | flops 1611005952 | bytes 6029312 | tf_op jit(solution)/shard_map/dot_general | solution.py:724
  97.0 0.0 copy-start.3
  97.0 0.0 copy-start.6
  97.0 0.0 copy-start.1
  97.0 0.0 copy-start.5
  97.0 0.8 copy-done.3
  97.8 0.1 pad_convert_fusion.1
  97.9 0.7 constant_dynamic-slice_fusion.2
  98.6 0.2 multiply_convert_fusion.5
  98.8 0.0 copy-done.6
  98.8 0.1 dynamic_slice.32
  98.9 0.0 copy-done
  98.9 0.0 copy-done.1
  98.9 0.0 copy-done.5
  98.9 0.7 bitcast_subtract_fusion
  99.6 0.1 copy.69
  99.8 0.2 fusion.62
  100.0 0.0 slice-done
  100.0 0.1 pad_convert_fusion
  100.0 0.9 constant_dynamic-slice_fusion.1
  101.0 0.3 multiply_convert_fusion.3
  101.3 0.0 copy-start.4
  101.3 0.2 reshape.197
  101.6 0.3 copy.57
  101.8 0.1 copy.58
  101.9 0.1 bitcast_exponential_fusion
  102.0 0.2 multiply_convert_fusion.4
  102.3 0.5 convolution_bitcast_fusion.1
  102.8 0.0 copy-done.4
  102.8 0.8 while.13
  103.0 0.1 bitcast_add_fusion.2
  103.2 0.1 bitcast_add_fusion.2
  103.3 0.1 bitcast_add_fusion.2
  103.5 0.1 bitcast_add_fusion.2
  103.6 0.4 fusion.9
  104.0 0.1 copy.54
  104.1 0.2 fusion.63
  104.3 0.5 fusion.8
  104.9 0.4 copy.70
  105.3 0.6 reshape.195
  105.9 0.0 copy-start.2
  105.9 1.3 multiply_reduce_fusion
  107.3 1.1 broadcast_multiply_fusion
  108.4 0.8 dynamic_slice.34
  109.2 0.7 multiply_convert_fusion.2.mixer
  109.9 0.0 copy-done.2
  109.9 3.7 %convolution_convert_fusion = bf16[512,768]{1,0:T(8,128)(2,1)S(1)} fusion(bf16[512,2048]{1,0:T(8,128)(2,1)S(1)} %bitcast.139, bf16[2048,768]{1,0:T(8,128)(2,1)} %bitcast.154), kind=kOutput, calls=%fused_computation.14 | convolution fusion | flops 1611005952 | bytes 6029312 | tf_op jit(solution)/shard_map/dot_general | solution.py:724
  113.6 0.0 copy-start.7
  113.6 0.1 slice_bitcast_fusion.1
  113.7 0.1 copy.71
  113.9 0.4 copy-done.7
  114.3 0.1 dynamic_slice.35
  114.3 0.7 fusion.37
  115.0 0.1 iota_compare_fusion.1
  115.1 4.7 %select_convert_fusion = bf16[2,512,512]{2,1,0:T(8,128)(2,1)S(1)} fusion(f32[2,512,512]{2,1,0:T(8,128)S(1)} %get-tuple-element.112, f32[2]{0:T(128)S(1)} %dynamic_slice.35, pred[512,512]{1,0:T(8,128)(4,1)S(1)} %iota_compare_fusion.1, u8[512,512]{1,0:T(8,128)(4,1)S(1)} %get-tuple-element.111), kind=kOutput, calls=%fused_computation.7 | convolution fusion | flops 1627127808 | bytes 3670024 | tf_op jit(solution)/shard_map/htr,rs->hts/dot_general | solution.py:675
  119.8 0.5 fusion.10
  120.3 0.1 reshape.196
  120.4 0.9 copy.72.attend
  121.3 29.8 %shard_map.164 = bf16[64,2048]{1,0:T(8,128)(2,1)} custom-call(bf16[4,128,256]{2,1,0:T(8,128)(2,1)} %multiply_convert_fusion.2.mixer, bf16[4,128,256]{2,1,0:T(8,128)(2,1)} %copy.72.attend, bf16[512,2048]{1,0:T(8,128)(2,1)} %get-tuple-element.42.rows), custom_call_target="tpu_custom_call" | custom-call | tf_op jit(solution)/shard_map/pallas_call | solution.py:650
  151.1 1.7 %copy.101 = bf16[1,64,2048]{2,1,0:T(8,128)(2,1)} copy(bf16[1,64,2048]{2,1,0:T(8,128)(2,1)} %bitcast.146) | data formatting | bytes 524288
  (20 shorter events, 0.2 us)
Async XLA Ops:
  0.0 98.9 %copy-start = (bf16[2048,32]{0,1:T(8,128)(2,1)S(1)}, bf16[2048,32]{0,1:T(8,128)(2,1)}, u32[]{:S(2)}) copy-start(bf16[2048,32]{0,1:T(8,128)(2,1)} %param.25) | copy-start | bytes 393220
  97.0 0.9 copy-start.3
  97.0 1.9 %copy-start.6 = (f32[32]{0:T(128)S(1)}, f32[32]{0:T(128)}, u32[]{:S(2)}) copy-start(f32[32]{0:T(128)} %param.27) | copy-start | bytes 388
  97.0 1.9 %copy-start.1 = (bf16[4,128,2048]{2,1,0:T(8,128)(2,1)S(1)}, bf16[4,128,2048]{2,1,0:T(8,128)(2,1)}, u32[]{:S(2)}) copy-start(bf16[4,128,2048]{2,1,0:T(8,128)(2,1)} %get-tuple-element.37) | copy-start | bytes 6291460
  97.0 1.9 %copy-start.5 = (f32[4,4,128]{2,1,0:T(4,128)S(1)}, f32[4,4,128]{2,1,0:T(4,128)}, u32[]{:S(2)}) copy-start(f32[4,4,128]{2,1,0:T(4,128)} %get-tuple-element.39) | copy-start | bytes 24580
  98.6 1.4 slice-start
  101.3 1.5 copy-start.4
  105.9 4.0 %copy-start.2 = (bf16[4,128,2048]{2,1,0:T(8,128)(2,1)S(1)}, bf16[4,128,2048]{2,1,0:T(8,128)(2,1)}, u32[]{:S(2)}) copy-start(bf16[4,128,2048]{2,1,0:T(8,128)(2,1)} %get-tuple-element.37) | copy-start | bytes 6291460
  113.6 0.7 copy-start.7
